TPU v7x, 32 devices: a whole 2x2x4 slice. The times are simulated.
32 devices in a mesh: sp: 8 (over z, x), tp: 4 (over y, core).
Axes of the slice: x: 2, y: 2, z: 4, core: 2. Of those that a mesh axis runs over, the one named last changes fastest.
Arguments:
- residual_in: bfloat16 [1536, 2048], P('sp', 'tp'), may hold values from -6 to 6
- query_rows: bfloat16 [1536, 1024], P('sp', 'tp'), may hold values from -8 to 8
- key_rows: bfloat16 [1536, 1024], P('sp', 'tp'), may hold values from -8 to 8
- value_rows: bfloat16 [1536, 1024], P('sp', 'tp'), may hold values from -6 to 6
- map_weight: float32 [16], P('tp'), may hold values from 0.3 to 0.8
- head_gain: float32 [64], replicated, may hold values from 0.1 to 1.9
- out_proj: bfloat16 [1024, 2048], P(None, 'tp'), may hold values from -0.1875 to 0.1875
- norm_gain: float32 [2048], replicated, may hold values from 0.1 to 1.9
- route_ids: int32 [1536, 2], P('sp'), may hold values from 0 to 7, all different within a row; in each aligned block of 192 rows (0 to 191, 192 to 383, ...) at most 60 rows name the same one
- route_weights: float32 [1536, 2], P('sp'), may hold values from 0.2 to 1.2
- expert_gate: bfloat16 [8, 1024, 2048], P('sp', 'tp'), may hold values from -0.125 to 0.125
- expert_up: bfloat16 [8, 1024, 2048], P('sp', 'tp'), may hold values from -0.125 to 0.125
- expert_down: bfloat16 [8, 1024, 2048], P('sp', None, 'tp'), may hold values from -0.1875 to 0.1875
- shared_gate: bfloat16 [1024, 2048], P('tp'), may hold values from -0.125 to 0.125
- shared_up: bfloat16 [1024, 2048], P('tp'), may hold values from -0.125 to 0.125
- shared_down: bfloat16 [1024, 2048], P(None, 'tp'), may hold values from -0.1875 to 0.1875
Outputs:
- mixed_out: bfloat16 [1536, 2048], P('sp', 'tp')
Inputs may be any that keep to these rules, and one draw needn't show every extreme that they name: `route_ids`: each row names 2 different experts. Among the rows held by one index of sp no expert is named more than 60 times, and in every draw some expert is named exactly 60 times by the rows of some index of sp.
All inputs are finite; a program needn't handle non-finite values.
Results may differ from a plain program's by a relative error of at most 0.0095.
Values may be sent and summed in bfloat16 or wider, within the bound.
A program may use at most 64 MiB of HBM per device.

v0:
```python
import functools

import jax
import jax.numpy as jnp
from jax import lax
from jax.experimental import pallas as pl
from jax.experimental.pallas import tpu as pltpu
from jax.sharding import PartitionSpec as P

epsilon = 1e-06
masked_score = -1e30
MESH = pl.DeviceIdType.MESH


def rms_scale(values, gain_vec):
    squares = jnp.mean(values * values, axis=-1, keepdims=True)
    return values * lax.rsqrt(squares + epsilon) * gain_vec


def block_slots(route_block, experts_all, capacity):
    flat_ids = route_block.reshape(-1)
    one_hot = (flat_ids[:, None] == jnp.arange(experts_all, dtype=jnp.int32)[None, :]).astype(
        jnp.int32
    )
    earlier = jnp.cumsum(one_hot, axis=0) - one_hot
    position = jnp.sum(earlier * one_hot, axis=1)
    return (flat_ids * capacity + position).reshape(route_block.shape)


def body(
    residual_in,
    query_rows,
    key_rows,
    value_rows,
    map_weight,
    head_gain,
    out_proj,
    norm_gain,
    route_ids,
    route_weights,
    expert_gate,
    expert_up,
    expert_down,
    shared_gate,
    shared_up,
    shared_down,
):
    seq_dev = residual_in.shape[0]
    col_dev = residual_in.shape[1]
    heads_here = map_weight.shape[0]
    head_dim = head_gain.shape[0]
    half_dim = head_dim // 2
    topk_count = route_ids.shape[1]
    exp_here = expert_gate.shape[0]
    experts_all = exp_here * lax.axis_size("sp")
    capacity = 5 * seq_dev * topk_count // (4 * experts_all)
    score_scale = half_dim ** (-0.5)
    query_pos = lax.axis_index("sp") * seq_dev + jnp.arange(seq_dev, dtype=jnp.int32)
    query_heads = query_rows.reshape(seq_dev, heads_here, 2, half_dim)
    key_piece = lax.all_gather(key_rows, "sp", axis=0, tiled=True)
    value_piece = lax.all_gather(value_rows, "sp", axis=0, tiled=True)
    piece_len = key_piece.shape[0]
    key_heads = key_piece.reshape(piece_len, heads_here, 2, half_dim)
    value_heads = value_piece.reshape(piece_len, heads_here, head_dim)
    scores = (
        jnp.einsum("qhmd,khmd->mhqk", query_heads, key_heads, preferred_element_type=jnp.float32)
        * score_scale
    )
    key_pos = jnp.arange(piece_len, dtype=jnp.int32)
    visible = key_pos[None, :] <= query_pos[:, None]
    scores = jnp.where(visible, scores, masked_score)
    run_max = jnp.full((2, heads_here, seq_dev), masked_score, jnp.float32)
    new_max = jnp.maximum(run_max, jnp.max(scores, axis=-1))
    expo = jnp.where(visible, jnp.exp(scores - new_max[..., None]), 0.0)
    new_sum = jnp.sum(expo, axis=-1)
    product = jnp.einsum(
        "mhqk,khd->mhqd", expo.astype(jnp.bfloat16), value_heads, preferred_element_type=jnp.float32
    )
    summed = product / new_sum[..., None]
    diff_out = summed[0] - map_weight[:, None, None] * summed[1]
    head_out = rms_scale(diff_out, head_gain).astype(jnp.bfloat16)
    head_out = jnp.transpose(head_out, (1, 0, 2)).reshape(seq_dev, heads_here * head_dim)
    attn = jnp.dot(
        lax.all_gather(head_out, "tp", axis=1, tiled=True),
        out_proj,
        preferred_element_type=jnp.float32,
    )
    hidden_state = (residual_in.astype(jnp.float32) + attn).astype(jnp.bfloat16)
    full_rows = lax.all_gather(hidden_state, "tp", axis=1, tiled=True)
    normed = rms_scale(full_rows.astype(jnp.float32), norm_gain).astype(jnp.bfloat16)
    shared_gate_part = jnp.einsum(
        "rd,fd->rf", normed, shared_gate, preferred_element_type=jnp.float32
    )
    shared_up_part = jnp.einsum("rd,fd->rf", normed, shared_up, preferred_element_type=jnp.float32)
    shared_hidden = (jax.nn.silu(shared_gate_part) * shared_up_part).astype(jnp.bfloat16)
    slot_ids = block_slots(route_ids, experts_all, capacity)
    token_of = jnp.repeat(jnp.arange(seq_dev, dtype=jnp.int32), topk_count)
    slot_token = (
        jnp.full((experts_all * capacity,), seq_dev, jnp.int32)
        .at[slot_ids.reshape(-1)]
        .set(token_of)
    )
    own_cols = lax.dynamic_slice_in_dim(normed, lax.axis_index("tp") * col_dev, col_dev, 1)
    padded = jnp.concatenate([own_cols, jnp.zeros((1, col_dev), jnp.bfloat16)], axis=0)
    outgoing = jnp.take(padded, slot_token, axis=0).reshape(experts_all, capacity, col_dev)
    arrived = lax.all_to_all(outgoing, "sp", split_axis=0, concat_axis=1, tiled=True)
    arrived_rows = arrived.shape[1]
    pieces = lax.all_gather(arrived, "tp", axis=2, tiled=True)
    gate_add = jnp.einsum("erd,efd->erf", pieces, expert_gate, preferred_element_type=jnp.float32)
    up_add = jnp.einsum("erd,efd->erf", pieces, expert_up, preferred_element_type=jnp.float32)
    expert_hidden = (jax.nn.silu(gate_add) * up_add).astype(jnp.bfloat16)
    expert_flat = expert_hidden.reshape(exp_here * arrived_rows, expert_hidden.shape[2])
    pieces = (
        lax.all_gather(shared_hidden, "tp", axis=1, tiled=True),
        lax.all_gather(expert_flat, "tp", axis=1, tiled=True),
    )
    piece_width = pieces[0].shape[1]
    routed_piece = pieces[1].reshape(exp_here, arrived_rows, piece_width)
    shared_add = jnp.dot(pieces[0], shared_down, preferred_element_type=jnp.float32)
    expert_add = jnp.einsum(
        "erf,efd->erd", routed_piece, expert_down, preferred_element_type=jnp.float32
    )
    returned_rows = lax.all_to_all(
        expert_add.astype(jnp.bfloat16), "sp", split_axis=1, concat_axis=0, tiled=True
    )
    returned_flat = returned_rows.reshape(experts_all * capacity, col_dev)
    picked = (
        jnp.take(returned_flat, slot_ids.reshape(-1), axis=0)
        .reshape(seq_dev, topk_count, col_dev)
        .astype(jnp.float32)
    )
    routed = jnp.sum(picked * route_weights[:, :, None], axis=1)
    return (hidden_state.astype(jnp.float32) + shared_add + routed).astype(jnp.bfloat16)


def lane_iota(rows):
    return lax.broadcasted_iota(jnp.int32, (rows, 128), 1)


def roll_half(values):
    return pltpu.roll(values, 64, 1)


def contract_last(a, b):
    return lax.dot_general(a, b, (((1,), (1,)), ((), ())), preferred_element_type=jnp.float32)


def layer_kernel(
    n_sp,
    n_tp,
    q_in,
    k_in,
    v_in,
    res_in,
    map_w,
    head_g,
    norm_g,
    ids_in,
    route_w,
    out_proj,
    exp_gate,
    exp_up,
    exp_down,
    sh_gate,
    sh_up,
    sh_down,
    out_ref,
    w_out,
    w_gate,
    w_up,
    w_down,
    w_sgate,
    w_sup,
    w_sdown,
    kv_out,
    q_out,
    kv_buf,
    q_buf,
    o_out,
    ho_buf,
    hid_buf,
    disp_out,
    arr_buf,
    sh_buf,
    eh_buf,
    res_out,
    ret_buf,
    spread_buf,
    pick_buf,
    weight_buf,
    w_sem,
    a_send,
    kv_recv,
    q_recv,
    o_send,
    o_recv,
    d_send,
    d_recv,
    r_send,
    r_recv,
    g_send,
    g_recv,
):
    me_s = lax.axis_index("sp")
    me_t = lax.axis_index("tp")
    sib = me_t + 1 - 2 * lax.rem(me_t, 2)
    peers = n_tp // 2 - 1
    rows = res_in.shape[0]
    col_dev = res_in.shape[1]
    half = rows // 2
    quarter = rows // 4
    cap = arr_buf.shape[2]
    half_dim = 32
    groups = eh_buf.shape[1]
    per_group = n_sp // groups
    bf16 = jnp.bfloat16
    f32 = jnp.float32

    def across(k):
        other = me_s
        for b in range(n_sp.bit_length() - 1):
            if k >> b & 1:
                bit = lax.rem(me_s // (1 << b), 2)
                other = other + (1 << b) * (1 - 2 * bit)
        return other

    loads = []
    for i, (src, dst) in enumerate(
        (
            (out_proj, w_out),
            (sh_gate, w_sgate),
            (sh_up, w_sup),
            (exp_gate.at[0], w_gate),
            (exp_up.at[0], w_up),
            (exp_down.at[0], w_down),
            (sh_down, w_sdown),
        )
    ):
        copy = pltpu.make_async_copy(src, dst, w_sem.at[i])
        copy.start()
        loads.append(copy)

    barrier = pltpu.get_barrier_semaphore()
    for d in range(1, n_sp):
        pl.semaphore_signal(
            barrier, inc=1, device_id={"sp": lax.rem(me_s + d, n_sp)}, device_id_type=MESH
        )
    for d in range(1, n_tp):
        pl.semaphore_signal(
            barrier, inc=1, device_id={"tp": lax.rem(me_t + d, n_tp)}, device_id_type=MESH
        )

    sends = []

    def send(src, dst, ssem, rsem, device):
        copy = pltpu.make_async_remote_copy(
            src_ref=src,
            dst_ref=dst,
            send_sem=ssem,
            recv_sem=rsem,
            device_id=device,
            device_id_type=MESH,
        )
        copy.start()
        return copy

    def wait_recv(ref, ssem, rsem, device):
        pltpu.make_async_remote_copy(
            src_ref=ref,
            dst_ref=ref,
            send_sem=ssem,
            recv_sem=rsem,
            device_id=device,
            device_id_type=MESH,
        ).wait_recv()

    n_gs = 1 + 2 * peers

    def gather_start(piece, get):
        for k in range(1, peers + 1):
            other = lax.rem(me_t + 2 * k, n_tp)
            sends.append(
                send(
                    get(me_t),
                    get(me_t),
                    g_send.at[piece * n_gs + k],
                    g_recv.at[piece * n_tp + me_t],
                    {"tp": other},
                )
            )
        sends.append(
            send(
                get(me_t),
                get(me_t),
                g_send.at[piece * n_gs],
                g_recv.at[piece * n_tp + me_t],
                {"tp": sib},
            )
        )

    def gather_relay(piece, get):
        for k in range(1, peers + 1):
            other = lax.rem(me_t + 2 * k, n_tp)
            wait_recv(
                get(other), g_send.at[piece * n_gs], g_recv.at[piece * n_tp + other], {"tp": sib}
            )
            sends.append(
                send(
                    get(other),
                    get(other),
                    g_send.at[piece * n_gs + peers + k],
                    g_recv.at[piece * n_tp + other],
                    {"tp": sib},
                )
            )

    def gather_finish(piece, get):
        for k in range(peers + 1):
            other = lax.rem(sib + 2 * k, n_tp)
            wait_recv(
                get(other), g_send.at[piece * n_gs], g_recv.at[piece * n_tp + other], {"tp": sib}
            )

    low_rows = lane_iota(rows) < 64
    low_quarter = lane_iota(quarter) < 64
    for j in range(n_sp // 4):
        pair = slice(j * 128, (j + 1) * 128)
        keys = k_in[:, pair].astype(f32)
        vals = v_in[:, pair].astype(f32)
        kv_out[2 * j] = jnp.where(low_rows, keys, roll_half(vals)).astype(bf16)
        kv_out[2 * j + 1] = jnp.where(low_rows, roll_half(keys), vals).astype(bf16)
        for p in range(2):
            first = q_in[p * half : p * half + quarter, pair].astype(f32)
            second = q_in[p * half + quarter : (p + 1) * half, pair].astype(f32)
            q_out[4 * j + p] = jnp.where(low_quarter, first, roll_half(second)).astype(bf16)
            q_out[4 * j + 2 + p] = jnp.where(low_quarter, roll_half(first), second).astype(bf16)

    pl.semaphore_wait(barrier, n_sp + n_tp - 2)

    for d in (6, 7, 4, 5, 2, 3, 1):
        dst = across(d)
        sends.append(
            send(
                kv_out.at[dst // 2],
                kv_buf.at[me_s],
                a_send.at[2 * d],
                kv_recv.at[me_s],
                {"sp": dst},
            )
        )
        sends.append(
            send(
                q_out.at[dst], q_buf.at[me_s], a_send.at[2 * d + 1], q_recv.at[me_s], {"sp": dst}
            )
        )
    kv_buf[me_s] = kv_out[me_s // 2]
    q_buf[me_s] = q_out[me_s]

    eye = lax.broadcasted_iota(jnp.int32, (rows, rows), 0)
    eye_lane = lax.broadcasted_iota(jnp.int32, (rows, rows), 1)
    same = eye == eye_lane
    before_col = eye_lane < eye
    before_row = eye < eye_lane

    def as_column(row):
        return jnp.sum(jnp.where(same, row, 0.0), axis=1, keepdims=True)

    ids_row = [jnp.bitwise_xor(ids_in[c : c + 1, :], me_s).astype(f32) for c in range(2)]
    ids_col = [as_column(row) for row in ids_row]
    weight_col = [as_column(route_w[c : c + 1, :]) for c in range(2)]
    slot_row = []
    slot_col = []
    for c in range(2):
        hit = (ids_row[0] == ids_col[c]) | (ids_row[1] == ids_col[c])
        count = jnp.sum(jnp.where(hit & before_col, 1.0, 0.0), axis=1, keepdims=True)
        slot_col.append(ids_col[c] * cap + count)
        hit = (ids_col[0] == ids_row[c]) | (ids_col[1] == ids_row[c])
        count = jnp.sum(jnp.where(hit & before_row, 1.0, 0.0), axis=0, keepdims=True)
        slot_row.append(ids_row[c] * cap + count)
    slots = n_sp * cap
    slot_iota = lax.broadcasted_iota(jnp.int32, (slots, rows), 0).astype(f32)
    chosen = (slot_iota == slot_row[0]) | (slot_iota == slot_row[1])
    spread_buf[...] = jnp.where(chosen, 1.0, 0.0).astype(bf16)
    col_iota = lax.broadcasted_iota(jnp.int32, (rows, slots), 1).astype(f32)
    for c in range(2):
        pick_buf[c] = jnp.where(col_iota == slot_col[c], 1.0, 0.0).astype(bf16)
        weight_buf[c] = jnp.broadcast_to(weight_col[c], (rows, 128))
    head_lane = lax.broadcasted_iota(jnp.int32, map_w.shape, 1)
    map_here = jnp.sum(
        jnp.where(head_lane == me_s // 2, map_w[...], 0.0), axis=1, keepdims=True
    )
    gain_here = jnp.concatenate([jnp.zeros((1, 64), f32), head_g[...]], axis=1)

    parity = lax.rem(me_s, 2)
    lane_q = lane_iota(quarter)
    scale = half_dim ** (-0.5)
    row_in = lax.broadcasted_iota(jnp.int32, (half, rows), 0) + parity * half
    visible_half = lax.broadcasted_iota(jnp.int32, (half, rows), 1) <= row_in
    visible = jnp.concatenate([visible_half.astype(f32)] * 2, axis=0) > 0.5
    high_lanes = lane_iota(half) >= 64
    zero_q = jnp.zeros((quarter, 128), f32)
    first_map = lane_q < 32
    second_map = (lane_q >= 32) & (lane_q < 64)
    batch = n_sp // 2
    for start in range(0, n_sp, batch):
        steps = range(start, start + batch)
        for s in steps:

            @pl.when(me_s != s)
            def _():
                wait_recv(kv_buf.at[s], a_send.at[0], kv_recv.at[s], {"sp": s})
                wait_recv(q_buf.at[s], a_send.at[1], q_recv.at[s], {"sp": s})

        queries = {}
        for s in steps:
            packed = q_buf[s].astype(f32)
            rolled = roll_half(packed)
            queries[s] = jnp.concatenate(
                [
                    jnp.where(first_map, packed, zero_q),
                    jnp.where(first_map, rolled, zero_q),
                    jnp.where(second_map, packed, zero_q),
                    jnp.where(second_map, rolled, zero_q),
                ],
                axis=0,
            ).astype(bf16)
        keys = {s: kv_buf[0 : s + 1].reshape((s + 1) * rows, 128) for s in steps}
        scores = {}
        for s in steps:
            raw = contract_last(queries[s], keys[s]) * scale
            diag = jnp.where(visible, raw[:, s * rows :], masked_score)
            scores[s] = jnp.concatenate([raw[:, : s * rows], diag], axis=1) if s else diag
        row_max = {s: jnp.max(scores[s], axis=1, keepdims=True) for s in steps}
        expo = {s: jnp.exp(scores[s] - row_max[s]) for s in steps}
        total = {s: jnp.sum(expo[s], axis=1, keepdims=True) for s in steps}
        acc = {
            s: jnp.dot(expo[s].astype(bf16), keys[s], preferred_element_type=f32) for s in steps
        }
        diff = {}
        for s in steps:
            summed = acc[s] / total[s]
            raw = summed[0:half] - map_here * summed[half:rows]
            diff[s] = jnp.where(high_lanes, raw, 0.0)
        for s in steps:
            squares = jnp.sum(diff[s] * diff[s], axis=1, keepdims=True) * (1.0 / 64.0)
            head = diff[s] * lax.rsqrt(squares + epsilon) * gain_here
            o_out[s] = (roll_half(head[0:quarter]) + head[quarter:half]).astype(bf16)

        for s in steps:

            @pl.when(me_s != s)
            def _():
                send(
                    o_out.at[s],
                    ho_buf.at[me_t, me_s],
                    o_send.at[s],
                    o_recv.at[me_s],
                    {"sp": s},
                )

            @pl.when(me_s == s)
            def _():
                ho_buf[me_t, s] = o_out[s]

    split = n_sp // 2
    near = me_s // split * split

    def get_near(t):
        return ho_buf.at[t, pl.ds(near, split)]

    def get_far(t):
        return ho_buf.at[t, pl.ds(split - near, split)]

    for d in range(1, n_sp):
        if d == split:
            gather_start(0, get_near)
        other = across(d)
        wait_recv(ho_buf.at[me_t, other], o_send.at[d], o_recv.at[other], {"sp": other})
    gather_start(3 + n_sp + groups, get_far)
    for piece, get in ((0, get_near), (3 + n_sp + groups, get_far)):
        gather_relay(piece, get)
    for piece, get in ((0, get_near), (3 + n_sp + groups, get_far)):
        gather_finish(piece, get)

    blocks = []
    for p in range(2):
        for u in range(2):
            parts = []
            for t in range(n_tp):
                for j in range(n_sp // 4):
                    even = ho_buf[t, 4 * j + p].astype(f32)
                    odd = ho_buf[t, 4 * j + 2 + p].astype(f32)
                    if u == 0:
                        part = jnp.where(low_quarter, even, roll_half(odd))
                    else:
                        part = jnp.where(low_quarter, roll_half(even), odd)
                    parts.append(part.astype(bf16))
            blocks.append(jnp.concatenate(parts, axis=1))
    heads = jnp.concatenate(blocks, axis=0)
    loads[0].wait()
    attn = jnp.dot(heads, w_out[...], preferred_element_type=f32)
    hidden = (res_in[...].astype(f32) + attn).astype(bf16)
    hid_buf[me_t] = hidden

    def get_hid(t):
        return hid_buf.at[t]

    gather_start(1, get_hid)

    outgoing = jnp.dot(spread_buf[cap:slots], hidden, preferred_element_type=f32).astype(bf16)
    disp_out[1:n_sp] = outgoing.reshape(n_sp - 1, cap, col_dev)
    for d in range(1, n_sp):
        sends.append(
            send(
                disp_out.at[d],
                arr_buf.at[me_t, d],
                d_send.at[d],
                d_recv.at[d],
                {"sp": across(d)},
            )
        )

    def get_arr(d):
        return lambda t: arr_buf.at[t, d]

    def normalise(pieces):
        full = [piece.astype(f32) for piece in pieces]
        squares = sum(jnp.sum(piece * piece, axis=1, keepdims=True) for piece in full)
        factor = lax.rsqrt(squares * (1.0 / (n_tp * col_dev)) + epsilon)
        return jnp.concatenate(
            [
                (piece * factor * norm_g[:, t * col_dev : (t + 1) * col_dev]).astype(bf16)
                for t, piece in enumerate(full)
            ],
            axis=1,
        )

    def gated(normed, gate, up):
        gate_part = contract_last(normed, gate[...])
        up_part = contract_last(normed, up[...])
        return (gate_part / (1.0 + jnp.exp(-gate_part)) * up_part).astype(bf16)

    def arrive(d):
        wait_recv(arr_buf.at[me_t, d], d_send.at[d], d_recv.at[d], {"sp": across(d)})
        gather_start(2 + d, get_arr(d))

    def relay(d):
        gather_relay(2 + d, get_arr(d))

    def get_sh(t):
        return sh_buf.at[t]

    def get_eh(g):
        return lambda t: eh_buf.at[t, g]

    piece_sh = 2 + n_sp
    piece_eh = 3 + n_sp

    def expert_up(g):
        ds = range(g * per_group, (g + 1) * per_group)
        for d in ds:
            if d:
                gather_finish(2 + d, get_arr(d))
        normed = normalise(
            [
                arr_buf[t, g * per_group : (g + 1) * per_group].reshape(per_group * cap, col_dev)
                for t in range(n_tp)
            ]
        )
        eh_buf[me_t, g] = gated(normed, w_gate, w_up)

    def expert_out(g):
        gather_finish(piece_eh + g, get_eh(g))
        joined = jnp.concatenate([eh_buf[t, g] for t in range(n_tp)], axis=1)
        result = jnp.dot(joined, w_down[...], preferred_element_type=f32).astype(bf16)
        res_out[g * per_group : (g + 1) * per_group] = result.reshape(per_group, cap, col_dev)
        for d in range(g * per_group, (g + 1) * per_group):
            if d == 0:
                ret_buf[0] = res_out[0]
            else:
                sends.append(
                    send(
                        res_out.at[d],
                        ret_buf.at[d],
                        r_send.at[d],
                        r_recv.at[d],
                        {"sp": across(d)},
                    )
                )

    def relay_eh(g):
        gather_relay(piece_eh + g, get_eh(g))

    def start_eh(g):
        gather_start(piece_eh + g, get_eh(g))

    def relay_eh(g):
        gather_relay(piece_eh + g, get_eh(g))

    arrive(1)
    arrive(2)
    gather_relay(1, get_hid)
    arrive(3)
    relay(1)
    relay(2)
    arrive(4)
    gather_finish(1, get_hid)
    loads[1].wait()
    loads[2].wait()
    normed_own = normalise([hid_buf[t] for t in range(n_tp)])
    sh_buf[me_t] = gated(normed_own, w_sgate, w_sup)
    relay(3)
    arrive(5)
    relay(4)
    for t in range(n_tp):
        arr_buf[t, 0] = jnp.dot(
            spread_buf[0:cap], hid_buf[t], preferred_element_type=f32
        ).astype(bf16)
    for i in range(3, 7):
        loads[i].wait()
    expert_up(0)
    arrive(6)
    relay(5)
    expert_up(2)
    start_eh(2)
    expert_up(1)
    arrive(7)
    start_eh(1)
    start_eh(0)
    relay(6)
    relay_eh(2)
    relay(7)
    expert_out(2)
    expert_up(3)
    start_eh(3)
    gather_start(piece_sh, get_sh)
    relay_eh(1)
    relay_eh(0)
    expert_out(1)
    expert_out(0)
    relay_eh(3)
    expert_out(3)
    gather_relay(piece_sh, get_sh)

    gather_finish(piece_sh, get_sh)
    shared_all = jnp.concatenate([sh_buf[t] for t in range(n_tp)], axis=1)
    result = hid_buf[me_t].astype(f32) + jnp.dot(
        shared_all, w_sdown[...], preferred_element_type=f32
    )
    for d in range(1, n_sp):
        wait_recv(ret_buf.at[d], r_send.at[d], r_recv.at[d], {"sp": across(d)})
    returned = ret_buf[...].reshape(slots, col_dev)
    for c in range(2):
        picked = jnp.dot(pick_buf[c], returned, preferred_element_type=f32)
        result = result + weight_buf[c][:, 0:1] * picked
    out_ref[...] = result.astype(out_ref.dtype)

    for copy in sends:
        copy.wait_send()
    for s in range(n_sp):

        @pl.when(me_s != s)
        def _():
            pltpu.make_async_remote_copy(
                src_ref=o_out.at[s],
                dst_ref=ho_buf.at[me_t, me_s],
                send_sem=o_send.at[s],
                recv_sem=o_recv.at[me_s],
                device_id={"sp": s},
                device_id_type=MESH,
            ).wait_send()


def fused_body(
    residual_in,
    query_rows,
    key_rows,
    value_rows,
    map_weight,
    head_gain,
    out_proj,
    norm_gain,
    route_ids,
    route_weights,
    expert_gate,
    expert_up,
    expert_down,
    shared_gate,
    shared_up,
    shared_down,
):
    n_sp = lax.axis_size("sp")
    n_tp = lax.axis_size("tp")
    rows, col_dev = residual_in.shape
    topk = route_ids.shape[1]
    capacity = 5 * rows * topk // (4 * n_sp)
    cap = (capacity + 15) // 16 * 16
    hid_units = shared_gate.shape[0]
    bf16 = jnp.bfloat16
    groups = n_sp // 2
    pieces = 4 + n_sp + groups
    n_gs = 1 + 2 * (n_tp // 2 - 1)
    dma = pltpu.SemaphoreType.DMA
    vmem = pl.BlockSpec(memory_space=pltpu.VMEM)
    hbm = pl.BlockSpec(memory_space=pl.ANY)
    return pl.pallas_call(
        functools.partial(layer_kernel, n_sp, n_tp),
        out_shape=jax.ShapeDtypeStruct((rows, col_dev), bf16),
        in_specs=[vmem] * 9 + [hbm] * 7,
        out_specs=vmem,
        scratch_shapes=[
            pltpu.VMEM(out_proj.shape, bf16),
            pltpu.VMEM(expert_gate.shape[1:], bf16),
            pltpu.VMEM(expert_up.shape[1:], bf16),
            pltpu.VMEM(expert_down.shape[1:], bf16),
            pltpu.VMEM(shared_gate.shape, bf16),
            pltpu.VMEM(shared_up.shape, bf16),
            pltpu.VMEM(shared_down.shape, bf16),
            pltpu.VMEM((n_sp // 2, rows, 128), bf16),
            pltpu.VMEM((n_sp, rows // 4, 128), bf16),
            pltpu.VMEM((n_sp, rows, 128), bf16),
            pltpu.VMEM((n_sp, rows // 4, 128), bf16),
            pltpu.VMEM((n_sp, rows // 4, 128), bf16),
            pltpu.VMEM((n_tp, n_sp, rows // 4, 128), bf16),
            pltpu.VMEM((n_tp, rows, col_dev), bf16),
            pltpu.VMEM((n_sp, cap, col_dev), bf16),
            pltpu.VMEM((n_tp, n_sp, cap, col_dev), bf16),
            pltpu.VMEM((n_tp, rows, hid_units), bf16),
            pltpu.VMEM((n_tp, groups, n_sp // groups * cap, hid_units), bf16),
            pltpu.VMEM((n_sp, cap, col_dev), bf16),
            pltpu.VMEM((n_sp, cap, col_dev), bf16),
            pltpu.VMEM((n_sp * cap, rows), bf16),
            pltpu.VMEM((2, rows, n_sp * cap), bf16),
            pltpu.VMEM((2, rows, 128), jnp.float32),
            dma((7,)),
            dma((2 * n_sp,)),
            dma((n_sp,)),
            dma((n_sp,)),
            dma((n_sp,)),
            dma((n_sp,)),
            dma((n_sp,)),
            dma((n_sp,)),
            dma((n_sp,)),
            dma((n_sp,)),
            dma((pieces * n_gs,)),
            dma((pieces * n_tp,)),
        ],
        compiler_params=pltpu.CompilerParams(collective_id=0, has_side_effects=True),
    )(
        query_rows,
        key_rows,
        value_rows,
        residual_in,
        map_weight[None, :],
        head_gain[None, :],
        norm_gain[None, :],
        route_ids.T,
        route_weights.T,
        out_proj,
        expert_gate,
        expert_up,
        expert_down,
        shared_gate,
        shared_up,
        shared_down,
    )


def layer(*args):
    residual_in, map_weight, head_gain, route_ids = args[0], args[4], args[5], args[8]
    fits = (
        2 * map_weight.shape[0] == lax.axis_size("sp") == 8
        and map_weight.shape[0] % 2 == 0
        and head_gain.shape[0] == 64
        and route_ids.shape[1] == 2
        and args[10].shape[0] == 1
        and residual_in.shape[0] % 64 == 0
        and residual_in.shape[1] % 128 == 0
        and args[13].shape[0] % 128 == 0
        and lax.axis_size("tp") % 2 == 0
    )
    return (fused_body if fits else body)(*args)


def solution(mesh):
    in_specs = (
        P("sp", "tp"),
        P("sp", "tp"),
        P("sp", "tp"),
        P("sp", "tp"),
        P("tp"),
        P(),
        P(None, "tp"),
        P(),
        P("sp", None),
        P("sp", None),
        P("sp", "tp", None),
        P("sp", "tp", None),
        P("sp", None, "tp"),
        P("tp", None),
        P("tp", None),
        P(None, "tp"),
    )
    out_specs = P("sp", "tp")
    return jax.shard_map(layer, mesh=mesh, in_specs=in_specs, out_specs=out_specs, check_vma=False)
```

profile of v0, /device:TPU:0, one launch (start us, length us, event | category | flops | bytes accessed | tf_op | source)
XLA Modules:
  0.0 69.3 jit_solution(146876330381917372)
XLA Ops:
  0.0 67.6 %shard_map.154 = bf16[192,512]{1,0:T(8,128)(2,1)} custom-call(bf16[192,256]{1,0:T(8,128)(2,1)} %q_in.1, bf16[192,256]{1,0:T(8,128)(2,1)} %k_in.1, bf16[192,256]{1,0:T(8,128)(2,1)} %v_in.1, bf16[192,512]{1,0:T(8,128)(2,1)} %res_in.1, f32[1,4]{1,0:T(1,128)} %bitcast.8, f32[1,64]{1,0:T(1,128)} %bitcast.9, f32[1,2048]{1,0:T(1,128)} %bitcast.5, ...), custom_call_target="tpu_custom_call" | custom-call | tf_op jit(solution)/shard_map/pallas_call | solution.py:706
  67.6 1.6 %copy.18 = bf16[192,512]{1,0:T(8,128)(2,1)} copy(bf16[192,512]{1,0:T(8,128)(2,1)} %shard_map.154) | data formatting | bytes 393216
where the time goes:
time: 69.8 us; the launch traced here: 69.3 us
  Pallas kernels  67.6 us (97%)
  local copies, waits for them, and re-layouts  1.62 us (2%)
    pallas_call x1, Pallas kernels, fused_body(): pl.pallas_call(functools.partial(layer_kernel, n_sp, n_tp), out_shape=jax...  67.6 us
    unnamed x1, local copies, waits for them, and re-layouts  1.62 us

commit v1 on v0

--- a/solution.py
+++ b/solution.py
@@ -200,6 +200,10 @@
     r_recv,
     g_send,
     g_recv,
+    peer_out,
+    p_send,
+    p_recv,
+    shared_sum,
 ):
     me_s = lax.axis_index("sp")
     me_t = lax.axis_index("tp")
@@ -211,8 +215,7 @@
     quarter = rows // 4
     cap = arr_buf.shape[2]
     half_dim = 32
-    groups = eh_buf.shape[1]
-    per_group = n_sp // groups
+    piece_far = 3 + 2 * n_sp
     bf16 = jnp.bfloat16
     f32 = jnp.float32
 
@@ -339,15 +342,18 @@
 
     for d in (6, 7, 4, 5, 2, 3, 1):
         dst = across(d)
-        sends.append(
-            send(
-                kv_out.at[dst // 2],
-                kv_buf.at[me_s],
-                a_send.at[2 * d],
-                kv_recv.at[me_s],
-                {"sp": dst},
-            )
-        )
+        if d % 2 == 0 or d == 1:
+            sends.append(
+                send(
+                    kv_out.at[dst // 2],
+                    kv_buf.at[me_s],
+                    a_send.at[2 * d],
+                    kv_recv.at[me_s],
+                    {"sp": dst},
+                )
+            )
+    for d in (6, 7, 4, 5, 2, 3, 1):
+        dst = across(d)
         sends.append(
             send(
                 q_out.at[dst], q_buf.at[me_s], a_send.at[2 * d + 1], q_recv.at[me_s], {"sp": dst}
@@ -402,15 +408,30 @@
     first_map = lane_q < 32
     second_map = (lane_q >= 32) & (lane_q < 64)
     batch = n_sp // 2
-    for start in range(0, n_sp, batch):
+    for d in (6, 4, 2):
+        src = across(d)
+        wait_recv(kv_buf.at[src], a_send.at[0], kv_recv.at[src], {"sp": src})
+        sends.append(
+            send(
+                kv_buf.at[src],
+                kv_buf.at[src],
+                a_send.at[2 * d + 2],
+                kv_recv.at[src],
+                {"sp": across(1)},
+            )
+        )
+    for s in range(n_sp):
+
+        @pl.when(parity != s % 2)
+        def _():
+            wait_recv(kv_buf.at[s], a_send.at[0], kv_recv.at[s], {"sp": across(1)})
+
+        @pl.when(me_s != s)
+        def _():
+            wait_recv(q_buf.at[s], a_send.at[1], q_recv.at[s], {"sp": s})
+
+    def attend(start):
         steps = range(start, start + batch)
-        for s in steps:
-
-            @pl.when(me_s != s)
-            def _():
-                wait_recv(kv_buf.at[s], a_send.at[0], kv_recv.at[s], {"sp": s})
-                wait_recv(q_buf.at[s], a_send.at[1], q_recv.at[s], {"sp": s})
-
         queries = {}
         for s in steps:
             packed = q_buf[s].astype(f32)
@@ -462,24 +483,36 @@
             def _():
                 ho_buf[me_t, s] = o_out[s]
 
+    upper = me_s // batch
+
+    @pl.when(upper == 1)
+    def _():
+        attend(0)
+        attend(batch)
+
+    @pl.when(upper == 0)
+    def _():
+        attend(batch)
+        attend(0)
+
     split = n_sp // 2
-    near = me_s // split * split
+    base = me_s // split * split
 
     def get_near(t):
-        return ho_buf.at[t, pl.ds(near, split)]
+        return ho_buf.at[t, pl.ds(base, split)]
 
     def get_far(t):
-        return ho_buf.at[t, pl.ds(split - near, split)]
-
-    for d in range(1, n_sp):
-        if d == split:
-            gather_start(0, get_near)
+        return ho_buf.at[t, pl.ds(split - base, split)]
+
+    for d in (4, 5, 6, 7, 1, 2, 3):
         other = across(d)
         wait_recv(ho_buf.at[me_t, other], o_send.at[d], o_recv.at[other], {"sp": other})
-    gather_start(3 + n_sp + groups, get_far)
-    for piece, get in ((0, get_near), (3 + n_sp + groups, get_far)):
+        if d == n_sp - 1:
+            gather_start(piece_far, get_far)
+    gather_start(0, get_near)
+    for piece, get in ((piece_far, get_far), (0, get_near)):
         gather_relay(piece, get)
-    for piece, get in ((0, get_near), (3 + n_sp + groups, get_far)):
+    for piece, get in ((piece_far, get_far), (0, get_near)):
         gather_finish(piece, get)
 
     blocks = []
@@ -507,17 +540,41 @@
 
     gather_start(1, get_hid)
 
-    outgoing = jnp.dot(spread_buf[cap:slots], hidden, preferred_element_type=f32).astype(bf16)
-    disp_out[1:n_sp] = outgoing.reshape(n_sp - 1, cap, col_dev)
-    for d in range(1, n_sp):
+    near = n_sp // 2
+
+    def spread(lo, hi, cols):
+        picked = jnp.dot(spread_buf[lo * cap : hi * cap], cols, preferred_element_type=f32)
+        return picked.astype(bf16).reshape(hi - lo, cap, col_dev)
+
+    inner = lax.rem(me_s // 2 + upper, 2)
+
+    def slot_at(d):
+        return d if d < near else near + 2 * inner + 1 - d % 2
+
+    def offset_of(e):
+        if e < near:
+            return e
+        return (6 - 2 * inner if e < 6 else 4 + 2 * inner) + 1 - e % 2
+
+    def source(e):
+        if e < near:
+            return across(e)
+        side = me_s % 2 if e % 2 else 1 - me_s % 2
+        return 2 * (3 * (1 - upper) if e < 6 else 2 - upper) + side
+
+    def dispatch(d):
+        e = slot_at(d)
         sends.append(
             send(
-                disp_out.at[d],
-                arr_buf.at[me_t, d],
-                d_send.at[d],
-                d_recv.at[d],
-                {"sp": across(d)},
-            )
+                disp_out.at[d], arr_buf.at[me_t, e], d_send.at[d], d_recv.at[e], {"sp": across(d)}
+            )
+        )
+
+    def dispatch_peer(d, k):
+        other = lax.rem(me_t + 2 * k, n_tp)
+        i = (k - 1) * near + d
+        return send(
+            peer_out.at[i], arr_buf.at[other, d], p_send.at[i], p_recv.at[i], {"sp": across(d)}
         )
 
     def get_arr(d):
@@ -541,112 +598,174 @@
         return (gate_part / (1.0 + jnp.exp(-gate_part)) * up_part).astype(bf16)
 
     def arrive(d):
-        wait_recv(arr_buf.at[me_t, d], d_send.at[d], d_recv.at[d], {"sp": across(d)})
+        wait_recv(arr_buf.at[me_t, d], d_send.at[d], d_recv.at[d], {"sp": source(d)})
         gather_start(2 + d, get_arr(d))
 
     def relay(d):
         gather_relay(2 + d, get_arr(d))
 
+    def arrive_near(d):
+        piece = 2 + d
+        get = get_arr(d)
+        wait_recv(get(me_t), d_send.at[d], d_recv.at[d], {"sp": across(d)})
+        sends.append(
+            send(
+                get(me_t),
+                get(me_t),
+                g_send.at[piece * n_gs],
+                g_recv.at[piece * n_tp + me_t],
+                {"tp": sib},
+            )
+        )
+
+    def arrive_peer(d):
+        piece = 2 + d
+        get = get_arr(d)
+        for k in range(1, peers + 1):
+            other = lax.rem(me_t + 2 * k, n_tp)
+            i = (k - 1) * near + d
+            wait_recv(get(other), p_send.at[i], p_recv.at[i], {"sp": across(d)})
+            sends.append(
+                send(
+                    get(other),
+                    get(other),
+                    g_send.at[piece * n_gs + peers + k],
+                    g_recv.at[piece * n_tp + other],
+                    {"tp": sib},
+                )
+            )
+
     def get_sh(t):
         return sh_buf.at[t]
 
-    def get_eh(g):
-        return lambda t: eh_buf.at[t, g]
+    def get_eh(lo, hi):
+        return lambda t: eh_buf.at[t, pl.ds(lo, hi - lo)]
 
     piece_sh = 2 + n_sp
     piece_eh = 3 + n_sp
 
-    def expert_up(g):
-        ds = range(g * per_group, (g + 1) * per_group)
-        for d in ds:
+    def expert_up(lo, hi):
+        for d in range(lo, hi):
             if d:
                 gather_finish(2 + d, get_arr(d))
-        normed = normalise(
-            [
-                arr_buf[t, g * per_group : (g + 1) * per_group].reshape(per_group * cap, col_dev)
-                for t in range(n_tp)
-            ]
-        )
-        eh_buf[me_t, g] = gated(normed, w_gate, w_up)
-
-    def expert_out(g):
-        gather_finish(piece_eh + g, get_eh(g))
-        joined = jnp.concatenate([eh_buf[t, g] for t in range(n_tp)], axis=1)
+        count = (hi - lo) * cap
+        normed = normalise([arr_buf[t, lo:hi].reshape(count, col_dev) for t in range(n_tp)])
+        hidden_units = gated(normed, w_gate, w_up)
+        eh_buf[me_t, lo:hi] = hidden_units.reshape(hi - lo, cap, hidden_units.shape[1])
+
+    def start_eh(lo, hi):
+        gather_start(piece_eh + lo, get_eh(lo, hi))
+
+    def relay_eh(lo, hi):
+        gather_relay(piece_eh + lo, get_eh(lo, hi))
+
+    def expert_out(lo, hi):
+        gather_finish(piece_eh + lo, get_eh(lo, hi))
+        count = (hi - lo) * cap
+        joined = jnp.concatenate(
+            [eh_buf[t, lo:hi].reshape(count, eh_buf.shape[3]) for t in range(n_tp)], axis=1
+        )
         result = jnp.dot(joined, w_down[...], preferred_element_type=f32).astype(bf16)
-        res_out[g * per_group : (g + 1) * per_group] = result.reshape(per_group, cap, col_dev)
-        for d in range(g * per_group, (g + 1) * per_group):
+        res_out[lo:hi] = result.reshape(hi - lo, cap, col_dev)
+        for d in range(lo, hi):
             if d == 0:
                 ret_buf[0] = res_out[0]
             else:
                 sends.append(
                     send(
                         res_out.at[d],
-                        ret_buf.at[d],
+                        ret_buf.at[offset_of(d)],
                         r_send.at[d],
-                        r_recv.at[d],
-                        {"sp": across(d)},
+                        r_recv.at[offset_of(d)],
+                        {"sp": source(d)},
                     )
                 )
 
-    def relay_eh(g):
-        gather_relay(piece_eh + g, get_eh(g))
-
-    def start_eh(g):
-        gather_start(piece_eh + g, get_eh(g))
-
-    def relay_eh(g):
-        gather_relay(piece_eh + g, get_eh(g))
-
-    arrive(1)
-    arrive(2)
+    def shared_up():
+        normed_own = normalise([hid_buf[t] for t in range(n_tp)])
+        sh_buf[me_t] = gated(normed_own, w_sgate, w_sup)
+
+    def shared_down():
+        shared_all = jnp.concatenate([sh_buf[t] for t in range(n_tp)], axis=1)
+        shared_sum[...] = hid_buf[me_t].astype(f32) + jnp.dot(
+            shared_all, w_sdown[...], preferred_element_type=f32
+        )
+
+    def own_rows():
+        for t in range(n_tp):
+            arr_buf[t, 0] = jnp.dot(
+                spread_buf[0:cap], hid_buf[t], preferred_element_type=f32
+            ).astype(bf16)
+
+    def wait_loads():
+        for copy in loads[1:]:
+            copy.wait()
+
+    def send_own():
+        disp_out[near:n_sp] = spread(near, n_sp, hidden)
+        for d in (4, 6, 5, 7):
+            dispatch(d)
+        disp_out[1:near] = spread(1, near, hidden)
+        for d in range(1, near):
+            dispatch(d)
+
+    def peer_cols():
+        for k in range(1, peers + 1):
+            other = lax.rem(me_t + 2 * k, n_tp)
+            peer_out[(k - 1) * near + 1 : k * near] = spread(1, near, hid_buf[other])
+            for d in range(1, near):
+                sends.append(dispatch_peer(d, k))
+
+    send_own()
+    arrive(5)
     gather_relay(1, get_hid)
-    arrive(3)
-    relay(1)
-    relay(2)
+    peer_cols()
+    gather_finish(1, get_hid)
     arrive(4)
-    gather_finish(1, get_hid)
-    loads[1].wait()
-    loads[2].wait()
-    normed_own = normalise([hid_buf[t] for t in range(n_tp)])
-    sh_buf[me_t] = gated(normed_own, w_sgate, w_sup)
-    relay(3)
-    arrive(5)
+    relay(5)
+    wait_loads()
+    shared_up()
+    expert_up(5, 6)
+    start_eh(5, 6)
     relay(4)
-    for t in range(n_tp):
-        arr_buf[t, 0] = jnp.dot(
-            spread_buf[0:cap], hid_buf[t], preferred_element_type=f32
-        ).astype(bf16)
-    for i in range(3, 7):
-        loads[i].wait()
-    expert_up(0)
+    own_rows()
+    arrive(7)
+    arrive_near(1)
+    arrive_peer(1)
+    expert_up(4, 5)
+    start_eh(4, 5)
+    relay_eh(5, 6)
     arrive(6)
-    relay(5)
-    expert_up(2)
-    start_eh(2)
-    expert_up(1)
-    arrive(7)
-    start_eh(1)
-    start_eh(0)
+    gather_start(piece_sh, get_sh)
+    relay(7)
+    expert_up(0, 2)
+    expert_out(5, 6)
+    expert_up(7, 8)
+    start_eh(7, 8)
+    relay_eh(4, 5)
+    arrive_near(2)
+    arrive_near(3)
+    arrive_peer(2)
+    arrive_peer(3)
     relay(6)
-    relay_eh(2)
-    relay(7)
-    expert_out(2)
-    expert_up(3)
-    start_eh(3)
-    gather_start(piece_sh, get_sh)
-    relay_eh(1)
-    relay_eh(0)
-    expert_out(1)
-    expert_out(0)
-    relay_eh(3)
-    expert_out(3)
+    expert_out(4, 5)
+    start_eh(0, 2)
+    expert_up(6, 7)
+    start_eh(6, 7)
+    relay_eh(7, 8)
+    expert_up(2, 4)
+    start_eh(2, 4)
+    expert_out(7, 8)
+    relay_eh(0, 2)
     gather_relay(piece_sh, get_sh)
-
+    relay_eh(6, 7)
+    expert_out(0, 2)
+    expert_out(6, 7)
+    relay_eh(2, 4)
     gather_finish(piece_sh, get_sh)
-    shared_all = jnp.concatenate([sh_buf[t] for t in range(n_tp)], axis=1)
-    result = hid_buf[me_t].astype(f32) + jnp.dot(
-        shared_all, w_sdown[...], preferred_element_type=f32
-    )
+    shared_down()
+    expert_out(2, 4)
+    result = shared_sum[...]
     for d in range(1, n_sp):
         wait_recv(ret_buf.at[d], r_send.at[d], r_recv.at[d], {"sp": across(d)})
     returned = ret_buf[...].reshape(slots, col_dev)
@@ -697,8 +816,8 @@
     cap = (capacity + 15) // 16 * 16
     hid_units = shared_gate.shape[0]
     bf16 = jnp.bfloat16
-    groups = n_sp // 2
-    pieces = 4 + n_sp + groups
+    pieces = 4 + 2 * n_sp
+    peer_slots = (n_tp // 2 - 1) * (n_sp // 2)
     n_gs = 1 + 2 * (n_tp // 2 - 1)
     dma = pltpu.SemaphoreType.DMA
     vmem = pl.BlockSpec(memory_space=pltpu.VMEM)
@@ -726,7 +845,7 @@
             pltpu.VMEM((n_sp, cap, col_dev), bf16),
             pltpu.VMEM((n_tp, n_sp, cap, col_dev), bf16),
             pltpu.VMEM((n_tp, rows, hid_units), bf16),
-            pltpu.VMEM((n_tp, groups, n_sp // groups * cap, hid_units), bf16),
+            pltpu.VMEM((n_tp, n_sp, cap, hid_units), bf16),
             pltpu.VMEM((n_sp, cap, col_dev), bf16),
             pltpu.VMEM((n_sp, cap, col_dev), bf16),
             pltpu.VMEM((n_sp * cap, rows), bf16),
@@ -744,6 +863,10 @@
             dma((n_sp,)),
             dma((pieces * n_gs,)),
             dma((pieces * n_tp,)),
+            pltpu.VMEM((peer_slots, cap, col_dev), bf16),
+            dma((peer_slots,)),
+            dma((peer_slots,)),
+            pltpu.VMEM((rows, col_dev), jnp.float32),
         ],
         compiler_params=pltpu.CompilerParams(collective_id=0, has_side_effects=True),
     )(
@@ -777,7 +900,7 @@
         and residual_in.shape[0] % 64 == 0
         and residual_in.shape[1] % 128 == 0
         and args[13].shape[0] % 128 == 0
-        and lax.axis_size("tp") % 2 == 0
+        and lax.axis_size("tp") in (4, 8)
     )
     return (fused_body if fits else body)(*args)
 

time: 69.8 us -> 66.3 us (0.950)
  Pallas kernels: 67.6 us -> 64.5 us
    pallas_call x1, Pallas kernels: 67.6 us -> 64.5 us  [fused_body(): pl.pallas_call(functools.partial(layer_kernel, n_sp, n_tp), out_shape=jax...]
where the time goes in v1:
time: 66.3 us; the launch traced here: 66.1 us
  Pallas kernels  64.5 us (97%)
  local copies, waits for them, and re-layouts  1.62 us (2%)
    pallas_call x1, Pallas kernels, fused_body(): pl.pallas_call(functools.partial(layer_kernel, n_sp, n_tp), out_shape=jax...  64.5 us
    unnamed x1, local copies, waits for them, and re-layouts  1.62 us

profile of v1, /device:TPU:0, one launch (start us, length us, event | category | flops | bytes accessed | tf_op | source)
XLA Modules:
  0.0 66.1 jit_solution(16790413674603959342)
XLA Ops:
  0.0 64.5 %shard_map.154 = bf16[192,512]{1,0:T(8,128)(2,1)} custom-call(bf16[192,256]{1,0:T(8,128)(2,1)} %q_in.1, bf16[192,256]{1,0:T(8,128)(2,1)} %k_in.1, bf16[192,256]{1,0:T(8,128)(2,1)} %v_in.1, bf16[192,512]{1,0:T(8,128)(2,1)} %res_in.1, f32[1,4]{1,0:T(1,128)} %bitcast.8, f32[1,64]{1,0:T(1,128)} %bitcast.9, f32[1,2048]{1,0:T(1,128)} %bitcast.5, ...), custom_call_target="tpu_custom_call" | custom-call | tf_op jit(solution)/shard_map/pallas_call | solution.py:825
  64.5 1.6 %copy.18 = bf16[192,512]{1,0:T(8,128)(2,1)} copy(bf16[192,512]{1,0:T(8,128)(2,1)} %shard_map.154) | data formatting | bytes 393216

commit v2 on v1

--- a/solution.py
+++ b/solution.py
@@ -148,15 +148,15 @@
 def layer_kernel(
     n_sp,
     n_tp,
-    q_in,
-    k_in,
-    v_in,
-    res_in,
-    map_w,
-    head_g,
-    norm_g,
-    ids_in,
-    route_w,
+    q_hbm,
+    k_hbm,
+    v_hbm,
+    res_hbm,
+    map_w_hbm,
+    head_g_hbm,
+    norm_g_hbm,
+    ids_hbm,
+    route_w_hbm,
     out_proj,
     exp_gate,
     exp_up,
@@ -190,6 +190,7 @@
     weight_buf,
     w_sem,
     a_send,
+    q_send,
     kv_recv,
     q_recv,
     o_send,
@@ -204,6 +205,16 @@
     p_send,
     p_recv,
     shared_sum,
+    q_in,
+    k_in,
+    v_in,
+    res_in,
+    map_w,
+    head_g,
+    norm_g,
+    ids_in,
+    route_w,
+    in_sem,
 ):
     me_s = lax.axis_index("sp")
     me_t = lax.axis_index("tp")
@@ -227,6 +238,34 @@
                 other = other + (1 << b) * (1 - 2 * bit)
         return other
 
+    barrier = pltpu.get_barrier_semaphore()
+    for d in range(1, n_sp):
+        pl.semaphore_signal(
+            barrier, inc=1, device_id={"sp": lax.rem(me_s + d, n_sp)}, device_id_type=MESH
+        )
+    for d in range(1, n_tp):
+        pl.semaphore_signal(
+            barrier, inc=1, device_id={"tp": lax.rem(me_t + d, n_tp)}, device_id_type=MESH
+        )
+
+    inputs = []
+    for i, (src, dst) in enumerate(
+        (
+            (q_hbm, q_in),
+            (k_hbm, k_in),
+            (v_hbm, v_in),
+            (res_hbm, res_in),
+            (map_w_hbm, map_w),
+            (head_g_hbm, head_g),
+            (norm_g_hbm, norm_g),
+            (ids_hbm, ids_in),
+            (route_w_hbm, route_w),
+        )
+    ):
+        copy = pltpu.make_async_copy(src, dst, in_sem.at[i])
+        copy.start()
+        inputs.append(copy)
+
     loads = []
     for i, (src, dst) in enumerate(
         (
@@ -242,16 +281,6 @@
         copy = pltpu.make_async_copy(src, dst, w_sem.at[i])
         copy.start()
         loads.append(copy)
-
-    barrier = pltpu.get_barrier_semaphore()
-    for d in range(1, n_sp):
-        pl.semaphore_signal(
-            barrier, inc=1, device_id={"sp": lax.rem(me_s + d, n_sp)}, device_id_type=MESH
-        )
-    for d in range(1, n_tp):
-        pl.semaphore_signal(
-            barrier, inc=1, device_id={"tp": lax.rem(me_t + d, n_tp)}, device_id_type=MESH
-        )
 
     sends = []
 
@@ -324,6 +353,8 @@
                 get(other), g_send.at[piece * n_gs], g_recv.at[piece * n_tp + other], {"tp": sib}
             )
 
+    for copy in inputs[:3]:
+        copy.wait()
     low_rows = lane_iota(rows) < 64
     low_quarter = lane_iota(quarter) < 64
     for j in range(n_sp // 4):
@@ -347,21 +378,31 @@
                 send(
                     kv_out.at[dst // 2],
                     kv_buf.at[me_s],
-                    a_send.at[2 * d],
+                    a_send.at[d],
                     kv_recv.at[me_s],
                     {"sp": dst},
                 )
             )
-    for d in (6, 7, 4, 5, 2, 3, 1):
-        dst = across(d)
-        sends.append(
+    def send_queries(ds):
+        for d in ds:
+            dst = across(d)
             send(
-                q_out.at[dst], q_buf.at[me_s], a_send.at[2 * d + 1], q_recv.at[me_s], {"sp": dst}
-            )
-        )
+                q_out.at[dst], q_buf.at[me_s], q_send.at[d], q_recv.at[me_s], {"sp": dst}
+            )
+
+    upper = me_s // (n_sp // 2)
+    inner = lax.rem(me_s // 2 + upper, 2)
+
+    @pl.when(inner == 1)
+    def _():
+        send_queries((6, 7, 4, 5))
+
+    send_queries((2, 3, 1))
     kv_buf[me_s] = kv_out[me_s // 2]
     q_buf[me_s] = q_out[me_s]
 
+    for copy in inputs[3:]:
+        copy.wait()
     eye = lax.broadcasted_iota(jnp.int32, (rows, rows), 0)
     eye_lane = lax.broadcasted_iota(jnp.int32, (rows, rows), 1)
     same = eye == eye_lane
@@ -415,11 +456,17 @@
             send(
                 kv_buf.at[src],
                 kv_buf.at[src],
-                a_send.at[2 * d + 2],
+                a_send.at[d + 1],
                 kv_recv.at[src],
                 {"sp": across(1)},
             )
         )
+        if d == 6:
+
+            @pl.when(inner == 0)
+            def _():
+                send_queries((6, 7, 4, 5))
+
     for s in range(n_sp):
 
         @pl.when(parity != s % 2)
@@ -428,7 +475,7 @@
 
         @pl.when(me_s != s)
         def _():
-            wait_recv(q_buf.at[s], a_send.at[1], q_recv.at[s], {"sp": s})
+            wait_recv(q_buf.at[s], q_send.at[0], q_recv.at[s], {"sp": s})
 
     def attend(start):
         steps = range(start, start + batch)
@@ -483,7 +530,6 @@
             def _():
                 ho_buf[me_t, s] = o_out[s]
 
-    upper = me_s // batch
 
     @pl.when(upper == 1)
     def _():
@@ -545,8 +591,6 @@
     def spread(lo, hi, cols):
         picked = jnp.dot(spread_buf[lo * cap : hi * cap], cols, preferred_element_type=f32)
         return picked.astype(bf16).reshape(hi - lo, cap, col_dev)
-
-    inner = lax.rem(me_s // 2 + upper, 2)
 
     def slot_at(d):
         return d if d < near else near + 2 * inner + 1 - d % 2
@@ -776,6 +820,15 @@
 
     for copy in sends:
         copy.wait_send()
+    for d in range(1, n_sp):
+        pltpu.make_async_remote_copy(
+            src_ref=q_out.at[d],
+            dst_ref=q_buf.at[me_s],
+            send_sem=q_send.at[d],
+            recv_sem=q_recv.at[me_s],
+            device_id={"sp": across(d)},
+            device_id_type=MESH,
+        ).wait_send()
     for s in range(n_sp):
 
         @pl.when(me_s != s)
@@ -824,8 +877,8 @@
     hbm = pl.BlockSpec(memory_space=pl.ANY)
     return pl.pallas_call(
         functools.partial(layer_kernel, n_sp, n_tp),
-        out_shape=jax.ShapeDtypeStruct((rows, col_dev), bf16),
-        in_specs=[vmem] * 9 + [hbm] * 7,
+        out_shape=pltpu.VMEM((rows, col_dev), bf16),
+        in_specs=[hbm] * 16,
         out_specs=vmem,
         scratch_shapes=[
             pltpu.VMEM(out_proj.shape, bf16),
@@ -852,7 +905,8 @@
             pltpu.VMEM((2, rows, n_sp * cap), bf16),
             pltpu.VMEM((2, rows, 128), jnp.float32),
             dma((7,)),
-            dma((2 * n_sp,)),
+            dma((n_sp,)),
+            dma((n_sp,)),
             dma((n_sp,)),
             dma((n_sp,)),
             dma((n_sp,)),
@@ -867,6 +921,16 @@
             dma((peer_slots,)),
             dma((peer_slots,)),
             pltpu.VMEM((rows, col_dev), jnp.float32),
+            pltpu.VMEM(query_rows.shape, bf16),
+            pltpu.VMEM(key_rows.shape, bf16),
+            pltpu.VMEM(value_rows.shape, bf16),
+            pltpu.VMEM(residual_in.shape, bf16),
+            pltpu.VMEM((1,) + map_weight.shape, jnp.float32),
+            pltpu.VMEM((1,) + head_gain.shape, jnp.float32),
+            pltpu.VMEM((1,) + norm_gain.shape, jnp.float32),
+            pltpu.VMEM((topk, rows), jnp.int32),
+            pltpu.VMEM((topk, rows), jnp.float32),
+            dma((9,)),
         ],
         compiler_params=pltpu.CompilerParams(collective_id=0, has_side_effects=True),
     )(

time: 66.3 us -> 63.1 us (0.952)
  Pallas kernels: 64.5 us -> 62.3 us
  local copies, waits for them, and re-layouts: 1.62 us -> 0.68 us
    pallas_call x1, Pallas kernels: 64.5 us -> 62.3 us  [fused_body(): pl.pallas_call(functools.partial(layer_kernel, n_sp, n_tp), out_shape=plt...]
    unnamed x1, local copies, waits for them, and re-layouts: 1.62 us -> 0.68 us
where the time goes in v2:
time: 63.1 us; the launch traced here: 62.9 us
  Pallas kernels  62.3 us (99%)
  local copies, waits for them, and re-layouts  0.68 us (1%)
    pallas_call x1, Pallas kernels, fused_body(): pl.pallas_call(functools.partial(layer_kernel, n_sp, n_tp), out_shape=plt...  62.3 us

profile of v2, /device:TPU:0, one launch (start us, length us, event | category | flops | bytes accessed | tf_op | source)
XLA Modules:
  0.0 62.9 jit_solution(14016828948209219504)
XLA Ops:
  0.0 62.3 %shard_map.154 = bf16[192,512]{1,0:T(8,128)(2,1)S(1)} custom-call(bf16[192,256]{1,0:T(8,128)(2,1)} %q_hbm.1, bf16[192,256]{1,0:T(8,128)(2,1)} %k_hbm.1, bf16[192,256]{1,0:T(8,128)(2,1)} %v_hbm.1, bf16[192,512]{1,0:T(8,128)(2,1)} %res_hbm.1, f32[1,4]{1,0:T(1,128)} %bitcast.8, f32[1,64]{1,0:T(1,128)} %bitcast.9, f32[1,2048]{1,0:T(1,128)} %bitcast.5, ...), custom_call_target="tpu_custom_call" | custom-call | tf_op jit(solution)/shard_map/pallas_call | solution.py:878
  62.3 0.7 %copy.18 = bf16[192,512]{1,0:T(8,128)(2,1)} copy(bf16[192,512]{1,0:T(8,128)(2,1)S(1)} %shard_map.154) | data formatting | bytes 393216

commit v3 on v2

--- a/solution.py
+++ b/solution.py
@@ -215,6 +215,10 @@
     ids_in,
     route_w,
     in_sem,
+    t_gate,
+    t_up,
+    t_sgate,
+    t_sup,
 ):
     me_s = lax.axis_index("sp")
     me_t = lax.axis_index("tp")
@@ -467,6 +471,9 @@
             def _():
                 send_queries((6, 7, 4, 5))
 
+    for i, (src, dst) in ((3, (w_gate, t_gate)), (4, (w_up, t_up))):
+        loads[i].wait()
+        dst[...] = src[...].T
     for s in range(n_sp):
 
         @pl.when(parity != s % 2)
@@ -476,6 +483,20 @@
         @pl.when(me_s != s)
         def _():
             wait_recv(q_buf.at[s], q_send.at[0], q_recv.at[s], {"sp": s})
+
+    def send_rows(s, k, start=True):
+        copy = pltpu.make_async_remote_copy(
+            src_ref=o_out.at[s],
+            dst_ref=ho_buf.at[me_t, me_s],
+            send_sem=o_send.at[k * n_sp + s],
+            recv_sem=o_recv.at[k * n_sp + me_s],
+            device_id={"sp": s, "tp": lax.rem(me_t + 2 * k, n_tp)},
+            device_id_type=MESH,
+        )
+        if start:
+            copy.start()
+        else:
+            copy.wait_send()
 
     def attend(start):
         steps = range(start, start + batch)
@@ -518,13 +539,8 @@
 
             @pl.when(me_s != s)
             def _():
-                send(
-                    o_out.at[s],
-                    ho_buf.at[me_t, me_s],
-                    o_send.at[s],
-                    o_recv.at[me_s],
-                    {"sp": s},
-                )
+                for k in range(peers + 1):
+                    send_rows(s, k)
 
             @pl.when(me_s == s)
             def _():
@@ -550,16 +566,52 @@
     def get_far(t):
         return ho_buf.at[t, pl.ds(split - base, split)]
 
-    for d in (4, 5, 6, 7, 1, 2, 3):
-        other = across(d)
-        wait_recv(ho_buf.at[me_t, other], o_send.at[d], o_recv.at[other], {"sp": other})
-        if d == n_sp - 1:
-            gather_start(piece_far, get_far)
-    gather_start(0, get_near)
-    for piece, get in ((piece_far, get_far), (0, get_near)):
-        gather_relay(piece, get)
-    for piece, get in ((piece_far, get_far), (0, get_near)):
-        gather_finish(piece, get)
+    for i, (src, dst) in ((1, (w_sgate, t_sgate)), (2, (w_sup, t_sup))):
+        loads[i].wait()
+        dst[...] = src[...].T
+    for k in range(1, peers + 1):
+        sends.append(
+            send(
+                ho_buf.at[me_t, me_s],
+                ho_buf.at[me_t, me_s],
+                g_send.at[k],
+                o_recv.at[k * n_sp + me_s],
+                {"tp": lax.rem(me_t + 2 * k, n_tp)},
+            )
+        )
+
+    def wait_rows(d, k):
+        other = across(d) if d else me_s
+        from_t = lax.rem(me_t + 2 * k, n_tp)
+        wait_recv(
+            ho_buf.at[from_t, other],
+            o_send.at[0],
+            o_recv.at[k * n_sp + other],
+            {"sp": other, "tp": from_t},
+        )
+
+    def pass_on(piece, get, k):
+        from_t = lax.rem(me_t + 2 * k, n_tp)
+        sends.append(
+            send(
+                get(from_t),
+                get(from_t),
+                g_send.at[piece * n_gs + (peers + k if k else 0)],
+                g_recv.at[piece * n_tp + from_t],
+                {"tp": sib},
+            )
+        )
+
+    for k in range(peers + 1):
+        for d in range(split, n_sp):
+            wait_rows(d, k)
+        pass_on(piece_far, get_far, k)
+    for k in range(peers + 1):
+        for d in range(0 if k else 1, split):
+            wait_rows(d, k)
+        pass_on(0, get_near, k)
+    gather_finish(piece_far, get_far)
+    gather_finish(0, get_near)
 
     blocks = []
     for p in range(2):
@@ -637,8 +689,8 @@
         )
 
     def gated(normed, gate, up):
-        gate_part = contract_last(normed, gate[...])
-        up_part = contract_last(normed, up[...])
+        gate_part = jnp.dot(normed, gate[...], preferred_element_type=f32)
+        up_part = jnp.dot(normed, up[...], preferred_element_type=f32)
         return (gate_part / (1.0 + jnp.exp(-gate_part)) * up_part).astype(bf16)
 
     def arrive(d):
@@ -694,7 +746,7 @@
                 gather_finish(2 + d, get_arr(d))
         count = (hi - lo) * cap
         normed = normalise([arr_buf[t, lo:hi].reshape(count, col_dev) for t in range(n_tp)])
-        hidden_units = gated(normed, w_gate, w_up)
+        hidden_units = gated(normed, t_gate, t_up)
         eh_buf[me_t, lo:hi] = hidden_units.reshape(hi - lo, cap, hidden_units.shape[1])
 
     def start_eh(lo, hi):
@@ -727,7 +779,7 @@
 
     def shared_up():
         normed_own = normalise([hid_buf[t] for t in range(n_tp)])
-        sh_buf[me_t] = gated(normed_own, w_sgate, w_sup)
+        sh_buf[me_t] = gated(normed_own, t_sgate, t_sup)
 
     def shared_down():
         shared_all = jnp.concatenate([sh_buf[t] for t in range(n_tp)], axis=1)
@@ -742,7 +794,7 @@
             ).astype(bf16)
 
     def wait_loads():
-        for copy in loads[1:]:
+        for copy in loads[5:]:
             copy.wait()
 
     def send_own():
@@ -771,44 +823,44 @@
     shared_up()
     expert_up(5, 6)
     start_eh(5, 6)
+    own_rows()
     relay(4)
-    own_rows()
     arrive(7)
-    arrive_near(1)
-    arrive_peer(1)
     expert_up(4, 5)
     start_eh(4, 5)
     relay_eh(5, 6)
     arrive(6)
-    gather_start(piece_sh, get_sh)
+    arrive_near(1)
+    arrive_near(2)
+    arrive_near(3)
+    arrive_peer(1)
+    expert_out(5, 6)
+    arrive_peer(2)
+    arrive_peer(3)
     relay(7)
     expert_up(0, 2)
-    expert_out(5, 6)
+    start_eh(0, 2)
+    relay_eh(4, 5)
     expert_up(7, 8)
     start_eh(7, 8)
-    relay_eh(4, 5)
-    arrive_near(2)
-    arrive_near(3)
-    arrive_peer(2)
-    arrive_peer(3)
+    expert_out(4, 5)
     relay(6)
-    expert_out(4, 5)
-    start_eh(0, 2)
+    expert_up(2, 4)
+    start_eh(2, 4)
     expert_up(6, 7)
     start_eh(6, 7)
+    gather_start(piece_sh, get_sh)
+    relay_eh(0, 2)
     relay_eh(7, 8)
-    expert_up(2, 4)
-    start_eh(2, 4)
+    expert_out(0, 2)
     expert_out(7, 8)
-    relay_eh(0, 2)
+    relay_eh(2, 4)
+    relay_eh(6, 7)
+    expert_out(2, 4)
+    expert_out(6, 7)
     gather_relay(piece_sh, get_sh)
-    relay_eh(6, 7)
-    expert_out(0, 2)
-    expert_out(6, 7)
-    relay_eh(2, 4)
     gather_finish(piece_sh, get_sh)
     shared_down()
-    expert_out(2, 4)
     result = shared_sum[...]
     for d in range(1, n_sp):
         wait_recv(ret_buf.at[d], r_send.at[d], r_recv.at[d], {"sp": across(d)})
@@ -833,14 +885,8 @@
 
         @pl.when(me_s != s)
         def _():
-            pltpu.make_async_remote_copy(
-                src_ref=o_out.at[s],
-                dst_ref=ho_buf.at[me_t, me_s],
-                send_sem=o_send.at[s],
-                recv_sem=o_recv.at[me_s],
-                device_id={"sp": s},
-                device_id_type=MESH,
-            ).wait_send()
+            for k in range(peers + 1):
+                send_rows(s, k, start=False)
 
 
 def fused_body(
@@ -909,8 +955,8 @@
             dma((n_sp,)),
             dma((n_sp,)),
             dma((n_sp,)),
-            dma((n_sp,)),
-            dma((n_sp,)),
+            dma((n_tp // 2 * n_sp,)),
+            dma((n_tp // 2 * n_sp,)),
             dma((n_sp,)),
             dma((n_sp,)),
             dma((n_sp,)),
@@ -931,6 +977,10 @@
             pltpu.VMEM((topk, rows), jnp.int32),
             pltpu.VMEM((topk, rows), jnp.float32),
             dma((9,)),
+            pltpu.VMEM(expert_gate.shape[:0:-1], bf16),
+            pltpu.VMEM(expert_up.shape[:0:-1], bf16),
+            pltpu.VMEM(shared_gate.shape[::-1], bf16),
+            pltpu.VMEM(shared_up.shape[::-1], bf16),
         ],
         compiler_params=pltpu.CompilerParams(collective_id=0, has_side_effects=True),
     )(

time: 63.1 us -> 57.9 us (0.918)
  Pallas kernels: 62.3 us -> 56.7 us
    pallas_call x1, Pallas kernels: 62.3 us -> 56.7 us  [fused_body(): pl.pallas_call(functools.partial(layer_kernel, n_sp, n_tp), out_shape=plt...]
where the time goes in v3:
time: 57.9 us; the launch traced here: 57.4 us
  Pallas kernels  56.7 us (98%)
  local copies, waits for them, and re-layouts  0.68 us (1%)
    pallas_call x1, Pallas kernels, fused_body(): pl.pallas_call(functools.partial(layer_kernel, n_sp, n_tp), out_shape=plt...  56.7 us

profile of v3, /device:TPU:0, one launch (start us, length us, event | category | flops | bytes accessed | tf_op | source)
XLA Modules:
  0.0 57.4 jit_solution(11225289739952221696)
XLA Ops:
  0.0 56.7 %shard_map.154 = bf16[192,512]{1,0:T(8,128)(2,1)S(1)} custom-call(bf16[192,256]{1,0:T(8,128)(2,1)} %q_hbm.1, bf16[192,256]{1,0:T(8,128)(2,1)} %k_hbm.1, bf16[192,256]{1,0:T(8,128)(2,1)} %v_hbm.1, bf16[192,512]{1,0:T(8,128)(2,1)} %res_hbm.1, f32[1,4]{1,0:T(1,128)} %bitcast.8, f32[1,64]{1,0:T(1,128)} %bitcast.9, f32[1,2048]{1,0:T(1,128)} %bitcast.5, ...), custom_call_target="tpu_custom_call" | custom-call | tf_op jit(solution)/shard_map/pallas_call | solution.py:924
  56.7 0.7 %copy.18 = bf16[192,512]{1,0:T(8,128)(2,1)} copy(bf16[192,512]{1,0:T(8,128)(2,1)S(1)} %shard_map.154) | data formatting | bytes 393216

commit v4 on v3

--- a/solution.py
+++ b/solution.py
@@ -9,6 +9,7 @@
 
 epsilon = 1e-06
 masked_score = -1e30
+log2_e = 1.4426950408889634
 MESH = pl.DeviceIdType.MESH
 
 
@@ -189,21 +190,15 @@
     pick_buf,
     weight_buf,
     w_sem,
-    a_send,
-    q_send,
+    s_sem,
     kv_recv,
     q_recv,
-    o_send,
     o_recv,
-    d_send,
     d_recv,
-    r_send,
     r_recv,
-    g_send,
     g_recv,
+    p_recv,
     peer_out,
-    p_send,
-    p_recv,
     shared_sum,
     q_in,
     k_in,
@@ -230,7 +225,6 @@
     quarter = rows // 4
     cap = arr_buf.shape[2]
     half_dim = 32
-    piece_far = 3 + 2 * n_sp
     bf16 = jnp.bfloat16
     f32 = jnp.float32
 
@@ -266,7 +260,7 @@
             (route_w_hbm, route_w),
         )
     ):
-        copy = pltpu.make_async_copy(src, dst, in_sem.at[i])
+        copy = pltpu.make_async_copy(src, dst, in_sem.at[max(0, i - 2)])
         copy.start()
         inputs.append(copy)
 
@@ -286,79 +280,55 @@
         copy.start()
         loads.append(copy)
 
-    sends = []
-
     def send(src, dst, ssem, rsem, device):
-        copy = pltpu.make_async_remote_copy(
+        pltpu.make_async_remote_copy(
             src_ref=src,
             dst_ref=dst,
             send_sem=ssem,
             recv_sem=rsem,
             device_id=device,
             device_id_type=MESH,
-        )
-        copy.start()
-        return copy
-
-    def wait_recv(ref, ssem, rsem, device):
-        pltpu.make_async_remote_copy(
+        ).start()
+
+    def waiter(ref, ssem, rsem):
+        return pltpu.make_async_remote_copy(
             src_ref=ref,
             dst_ref=ref,
             send_sem=ssem,
             recv_sem=rsem,
-            device_id=device,
+            device_id={"tp": sib},
             device_id_type=MESH,
-        ).wait_recv()
-
-    n_gs = 1 + 2 * peers
-
-    def gather_start(piece, get):
+        )
+
+    def wait_recv(ref, rsem):
+        waiter(ref, s_sem.at[0], rsem).wait_recv()
+
+    def peer(k):
+        return lax.rem(me_t + 2 * k, n_tp)
+
+    def origin(k):
+        return lax.rem(me_t - 2 * k + n_tp, n_tp)
+
+    def channel(i, k):
+        return g_recv.at[i * (peers + 1) + k]
+
+    def pass_on(i, kind, block):
+        send(block, block, s_sem.at[kind], channel(i, 0), {"tp": sib})
+
+    def gather_start(i, kind, get):
         for k in range(1, peers + 1):
-            other = lax.rem(me_t + 2 * k, n_tp)
-            sends.append(
-                send(
-                    get(me_t),
-                    get(me_t),
-                    g_send.at[piece * n_gs + k],
-                    g_recv.at[piece * n_tp + me_t],
-                    {"tp": other},
-                )
-            )
-        sends.append(
-            send(
-                get(me_t),
-                get(me_t),
-                g_send.at[piece * n_gs],
-                g_recv.at[piece * n_tp + me_t],
-                {"tp": sib},
-            )
-        )
-
-    def gather_relay(piece, get):
+            send(get(me_t), get(me_t), s_sem.at[kind], channel(i, k), {"tp": peer(k)})
+        pass_on(i, kind, get(me_t))
+
+    def gather_relay(i, kind, get):
         for k in range(1, peers + 1):
-            other = lax.rem(me_t + 2 * k, n_tp)
-            wait_recv(
-                get(other), g_send.at[piece * n_gs], g_recv.at[piece * n_tp + other], {"tp": sib}
-            )
-            sends.append(
-                send(
-                    get(other),
-                    get(other),
-                    g_send.at[piece * n_gs + peers + k],
-                    g_recv.at[piece * n_tp + other],
-                    {"tp": sib},
-                )
-            )
-
-    def gather_finish(piece, get):
-        for k in range(peers + 1):
-            other = lax.rem(sib + 2 * k, n_tp)
-            wait_recv(
-                get(other), g_send.at[piece * n_gs], g_recv.at[piece * n_tp + other], {"tp": sib}
-            )
-
-    for copy in inputs[:3]:
-        copy.wait()
+            wait_recv(get(origin(k)), channel(i, k))
+            pass_on(i, kind, get(origin(k)))
+
+    def gather_finish(i, get):
+        wait_recv(get(pl.ds(0, peers + 1)), channel(i, 0))
+
+    pltpu.make_async_copy(kv_buf.at[0:6], kv_buf.at[0:6], in_sem.at[0]).wait()
     low_rows = lane_iota(rows) < 64
     low_quarter = lane_iota(quarter) < 64
     for j in range(n_sp // 4):
@@ -375,36 +345,20 @@
 
     pl.semaphore_wait(barrier, n_sp + n_tp - 2)
 
-    for d in (6, 7, 4, 5, 2, 3, 1):
+    for d in (6, 4, 2, 1):
         dst = across(d)
-        if d % 2 == 0 or d == 1:
-            sends.append(
-                send(
-                    kv_out.at[dst // 2],
-                    kv_buf.at[me_s],
-                    a_send.at[d],
-                    kv_recv.at[me_s],
-                    {"sp": dst},
-                )
-            )
+        send(kv_out.at[dst // 2], kv_buf.at[me_s], s_sem.at[0], kv_recv.at[d // 2], {"sp": dst})
+
     def send_queries(ds):
         for d in ds:
             dst = across(d)
-            send(
-                q_out.at[dst], q_buf.at[me_s], q_send.at[d], q_recv.at[me_s], {"sp": dst}
-            )
+            send(q_out.at[dst], q_buf.at[me_s], s_sem.at[1], q_recv.at[0], {"sp": dst})
 
     upper = me_s // (n_sp // 2)
     inner = lax.rem(me_s // 2 + upper, 2)
-
-    @pl.when(inner == 1)
-    def _():
-        send_queries((6, 7, 4, 5))
-
     send_queries((2, 3, 1))
     kv_buf[me_s] = kv_out[me_s // 2]
     q_buf[me_s] = q_out[me_s]
-
     for copy in inputs[3:]:
         copy.wait()
     eye = lax.broadcasted_iota(jnp.int32, (rows, rows), 0)
@@ -444,7 +398,9 @@
 
     parity = lax.rem(me_s, 2)
     lane_q = lane_iota(quarter)
-    scale = half_dim ** (-0.5)
+    scale = half_dim ** (-0.5) * log2_e
+    ones_lane = lane_iota(rows) == 0
+    one = jnp.ones((rows, 128), bf16)
     row_in = lax.broadcasted_iota(jnp.int32, (half, rows), 0) + parity * half
     visible_half = lax.broadcasted_iota(jnp.int32, (half, rows), 1) <= row_in
     visible = jnp.concatenate([visible_half.astype(f32)] * 2, axis=0) > 0.5
@@ -455,48 +411,24 @@
     batch = n_sp // 2
     for d in (6, 4, 2):
         src = across(d)
-        wait_recv(kv_buf.at[src], a_send.at[0], kv_recv.at[src], {"sp": src})
-        sends.append(
-            send(
-                kv_buf.at[src],
-                kv_buf.at[src],
-                a_send.at[d + 1],
-                kv_recv.at[src],
-                {"sp": across(1)},
-            )
-        )
+        wait_recv(kv_buf.at[src], kv_recv.at[d // 2])
+        send(kv_buf.at[src], kv_buf.at[src], s_sem.at[0], kv_recv.at[0], {"sp": across(1)})
         if d == 6:
-
-            @pl.when(inner == 0)
-            def _():
-                send_queries((6, 7, 4, 5))
-
+            send_queries((6, 7, 4, 5))
     for i, (src, dst) in ((3, (w_gate, t_gate)), (4, (w_up, t_up))):
         loads[i].wait()
         dst[...] = src[...].T
-    for s in range(n_sp):
-
-        @pl.when(parity != s % 2)
-        def _():
-            wait_recv(kv_buf.at[s], a_send.at[0], kv_recv.at[s], {"sp": across(1)})
-
-        @pl.when(me_s != s)
-        def _():
-            wait_recv(q_buf.at[s], q_send.at[0], q_recv.at[s], {"sp": s})
-
-    def send_rows(s, k, start=True):
-        copy = pltpu.make_async_remote_copy(
-            src_ref=o_out.at[s],
-            dst_ref=ho_buf.at[me_t, me_s],
-            send_sem=o_send.at[k * n_sp + s],
-            recv_sem=o_recv.at[k * n_sp + me_s],
-            device_id={"sp": s, "tp": lax.rem(me_t + 2 * k, n_tp)},
-            device_id_type=MESH,
-        )
-        if start:
-            copy.start()
-        else:
-            copy.wait_send()
+    wait_recv(kv_buf.at[0 : n_sp // 2], kv_recv.at[0])
+    wait_recv(q_buf.at[0 : n_sp - 1], q_recv.at[0])
+    def send_rows(s, k):
+        far = lax.rem(s // batch + upper, 2)
+        send(
+            o_out.at[s],
+            ho_buf.at[me_t, me_s],
+            s_sem.at[2],
+            o_recv.at[2 * k + far],
+            {"sp": s, "tp": peer(k)},
+        )
 
     def attend(start):
         steps = range(start, start + batch)
@@ -514,20 +446,19 @@
                 axis=0,
             ).astype(bf16)
         keys = {s: kv_buf[0 : s + 1].reshape((s + 1) * rows, 128) for s in steps}
+        blocks = [jnp.where(ones_lane, one, kv_buf[s]) for s in range(start + batch)]
+        values = {s: jnp.concatenate(blocks[: s + 1], axis=0) for s in steps}
         scores = {}
         for s in steps:
-            raw = contract_last(queries[s], keys[s]) * scale
+            raw = contract_last(queries[s], keys[s])
             diag = jnp.where(visible, raw[:, s * rows :], masked_score)
             scores[s] = jnp.concatenate([raw[:, : s * rows], diag], axis=1) if s else diag
         row_max = {s: jnp.max(scores[s], axis=1, keepdims=True) for s in steps}
-        expo = {s: jnp.exp(scores[s] - row_max[s]) for s in steps}
-        total = {s: jnp.sum(expo[s], axis=1, keepdims=True) for s in steps}
-        acc = {
-            s: jnp.dot(expo[s].astype(bf16), keys[s], preferred_element_type=f32) for s in steps
-        }
+        expo = {s: jnp.exp2(scores[s] * scale - row_max[s] * scale).astype(bf16) for s in steps}
+        acc = {s: jnp.dot(expo[s], values[s], preferred_element_type=f32) for s in steps}
         diff = {}
         for s in steps:
-            summed = acc[s] / total[s]
+            summed = acc[s] / acc[s][:, 0:1]
             raw = summed[0:half] - map_here * summed[half:rows]
             diff[s] = jnp.where(high_lanes, raw, 0.0)
         for s in steps:
@@ -570,55 +501,21 @@
         loads[i].wait()
         dst[...] = src[...].T
     for k in range(1, peers + 1):
-        sends.append(
-            send(
-                ho_buf.at[me_t, me_s],
-                ho_buf.at[me_t, me_s],
-                g_send.at[k],
-                o_recv.at[k * n_sp + me_s],
-                {"tp": lax.rem(me_t + 2 * k, n_tp)},
-            )
-        )
-
-    def wait_rows(d, k):
-        other = across(d) if d else me_s
-        from_t = lax.rem(me_t + 2 * k, n_tp)
-        wait_recv(
-            ho_buf.at[from_t, other],
-            o_send.at[0],
-            o_recv.at[k * n_sp + other],
-            {"sp": other, "tp": from_t},
-        )
-
-    def pass_on(piece, get, k):
-        from_t = lax.rem(me_t + 2 * k, n_tp)
-        sends.append(
-            send(
-                get(from_t),
-                get(from_t),
-                g_send.at[piece * n_gs + (peers + k if k else 0)],
-                g_recv.at[piece * n_tp + from_t],
-                {"tp": sib},
-            )
-        )
+        block = ho_buf.at[me_t, me_s]
+        send(block, block, s_sem.at[3], o_recv.at[2 * k], {"tp": peer(k)})
 
     for k in range(peers + 1):
-        for d in range(split, n_sp):
-            wait_rows(d, k)
-        pass_on(piece_far, get_far, k)
+        wait_recv(get_far(origin(k)), o_recv.at[2 * k + 1])
+        pass_on(0, 4, get_far(origin(k)))
     for k in range(peers + 1):
-        for d in range(0 if k else 1, split):
-            wait_rows(d, k)
-        pass_on(0, get_near, k)
-    gather_finish(piece_far, get_far)
-    gather_finish(0, get_near)
-
-    blocks = []
-    for p in range(2):
-        for u in range(2):
-            parts = []
-            for t in range(n_tp):
-                for j in range(n_sp // 4):
+        wait_recv(ho_buf.at[origin(k), 0 : split - (k == 0)], o_recv.at[2 * k])
+        pass_on(1, 4, get_near(origin(k)))
+    def project(j):
+        blocks = []
+        for p in range(2):
+            for u in range(2):
+                parts = []
+                for t in range(n_tp):
                     even = ho_buf[t, 4 * j + p].astype(f32)
                     odd = ho_buf[t, 4 * j + 2 + p].astype(f32)
                     if u == 0:
@@ -626,17 +523,27 @@
                     else:
                         part = jnp.where(low_quarter, roll_half(even), odd)
                     parts.append(part.astype(bf16))
-            blocks.append(jnp.concatenate(parts, axis=1))
-    heads = jnp.concatenate(blocks, axis=0)
+                blocks.append(jnp.concatenate(parts, axis=1))
+        heads = jnp.concatenate(blocks, axis=0)
+        wide = n_sp // 4 * 128
+        weights = jnp.concatenate(
+            [w_out[pl.ds(pl.multiple_of(t * wide + j * 128, 128), 128), :] for t in range(n_tp)],
+            axis=0,
+        )
+        return jnp.dot(heads, weights, preferred_element_type=f32)
+
     loads[0].wait()
-    attn = jnp.dot(heads, w_out[...], preferred_element_type=f32)
+    gather_finish(0, get_far)
+    attn = project(1 - upper)
+    gather_finish(1, get_near)
+    attn = attn + project(upper)
     hidden = (res_in[...].astype(f32) + attn).astype(bf16)
     hid_buf[me_t] = hidden
 
     def get_hid(t):
         return hid_buf.at[t]
 
-    gather_start(1, get_hid)
+    gather_start(2, 5, get_hid)
 
     near = n_sp // 2
 
@@ -660,17 +567,12 @@
 
     def dispatch(d):
         e = slot_at(d)
-        sends.append(
-            send(
-                disp_out.at[d], arr_buf.at[me_t, e], d_send.at[d], d_recv.at[e], {"sp": across(d)}
-            )
-        )
+        send(disp_out.at[d], arr_buf.at[me_t, e], s_sem.at[6], d_recv.at[e], {"sp": across(d)})
 
     def dispatch_peer(d, k):
-        other = lax.rem(me_t + 2 * k, n_tp)
-        i = (k - 1) * near + d
-        return send(
-            peer_out.at[i], arr_buf.at[other, d], p_send.at[i], p_recv.at[i], {"sp": across(d)}
+        i = (k - 1) * (near - 1) + d - 1
+        send(
+            peer_out.at[i], arr_buf.at[peer(k), d], s_sem.at[7], p_recv.at[i], {"sp": across(d)}
         )
 
     def get_arr(d):
@@ -693,43 +595,21 @@
         up_part = jnp.dot(normed, up[...], preferred_element_type=f32)
         return (gate_part / (1.0 + jnp.exp(-gate_part)) * up_part).astype(bf16)
 
-    def arrive(d):
-        wait_recv(arr_buf.at[me_t, d], d_send.at[d], d_recv.at[d], {"sp": source(d)})
-        gather_start(2 + d, get_arr(d))
-
-    def relay(d):
-        gather_relay(2 + d, get_arr(d))
+    def arrive(e):
+        wait_recv(arr_buf.at[me_t, e], d_recv.at[e])
+        gather_start(2 + e, 8, get_arr(e))
+
+    def relay(e):
+        gather_relay(2 + e, 8, get_arr(e))
 
     def arrive_near(d):
-        piece = 2 + d
-        get = get_arr(d)
-        wait_recv(get(me_t), d_send.at[d], d_recv.at[d], {"sp": across(d)})
-        sends.append(
-            send(
-                get(me_t),
-                get(me_t),
-                g_send.at[piece * n_gs],
-                g_recv.at[piece * n_tp + me_t],
-                {"tp": sib},
-            )
-        )
+        wait_recv(arr_buf.at[me_t, d], d_recv.at[d])
+        pass_on(2 + d, 9, arr_buf.at[me_t, d])
 
     def arrive_peer(d):
-        piece = 2 + d
-        get = get_arr(d)
         for k in range(1, peers + 1):
-            other = lax.rem(me_t + 2 * k, n_tp)
-            i = (k - 1) * near + d
-            wait_recv(get(other), p_send.at[i], p_recv.at[i], {"sp": across(d)})
-            sends.append(
-                send(
-                    get(other),
-                    get(other),
-                    g_send.at[piece * n_gs + peers + k],
-                    g_recv.at[piece * n_tp + other],
-                    {"tp": sib},
-                )
-            )
+            wait_recv(arr_buf.at[peer(k), d], p_recv.at[(k - 1) * (near - 1) + d - 1])
+            pass_on(2 + d, 9, arr_buf.at[peer(k), d])
 
     def get_sh(t):
         return sh_buf.at[t]
@@ -750,10 +630,10 @@
         eh_buf[me_t, lo:hi] = hidden_units.reshape(hi - lo, cap, hidden_units.shape[1])
 
     def start_eh(lo, hi):
-        gather_start(piece_eh + lo, get_eh(lo, hi))
+        gather_start(piece_eh + lo, 10, get_eh(lo, hi))
 
     def relay_eh(lo, hi):
-        gather_relay(piece_eh + lo, get_eh(lo, hi))
+        gather_relay(piece_eh + lo, 10, get_eh(lo, hi))
 
     def expert_out(lo, hi):
         gather_finish(piece_eh + lo, get_eh(lo, hi))
@@ -767,14 +647,12 @@
             if d == 0:
                 ret_buf[0] = res_out[0]
             else:
-                sends.append(
-                    send(
-                        res_out.at[d],
-                        ret_buf.at[offset_of(d)],
-                        r_send.at[d],
-                        r_recv.at[offset_of(d)],
-                        {"sp": source(d)},
-                    )
+                send(
+                    res_out.at[d],
+                    ret_buf.at[offset_of(d)],
+                    s_sem.at[11],
+                    r_recv.at[0],
+                    {"sp": source(d)},
                 )
 
     def shared_up():
@@ -798,8 +676,8 @@
             copy.wait()
 
     def send_own():
-        disp_out[near:n_sp] = spread(near, n_sp, hidden)
         for d in (4, 6, 5, 7):
+            disp_out[d : d + 1] = spread(d, d + 1, hidden)
             dispatch(d)
         disp_out[1:near] = spread(1, near, hidden)
         for d in range(1, near):
@@ -808,15 +686,15 @@
     def peer_cols():
         for k in range(1, peers + 1):
             other = lax.rem(me_t + 2 * k, n_tp)
-            peer_out[(k - 1) * near + 1 : k * near] = spread(1, near, hid_buf[other])
+            peer_out[(k - 1) * (near - 1) : k * (near - 1)] = spread(1, near, hid_buf[other])
             for d in range(1, near):
-                sends.append(dispatch_peer(d, k))
+                dispatch_peer(d, k)
 
     send_own()
     arrive(5)
-    gather_relay(1, get_hid)
+    gather_relay(2, 5, get_hid)
     peer_cols()
-    gather_finish(1, get_hid)
+    gather_finish(2, get_hid)
     arrive(4)
     relay(5)
     wait_loads()
@@ -824,8 +702,8 @@
     expert_up(5, 6)
     start_eh(5, 6)
     own_rows()
+    arrive(7)
     relay(4)
-    arrive(7)
     expert_up(4, 5)
     start_eh(4, 5)
     relay_eh(5, 6)
@@ -849,44 +727,45 @@
     start_eh(2, 4)
     expert_up(6, 7)
     start_eh(6, 7)
-    gather_start(piece_sh, get_sh)
+    gather_start(piece_sh, 12, get_sh)
     relay_eh(0, 2)
     relay_eh(7, 8)
     expert_out(0, 2)
     expert_out(7, 8)
     relay_eh(2, 4)
     relay_eh(6, 7)
+    expert_out(6, 7)
     expert_out(2, 4)
-    expert_out(6, 7)
-    gather_relay(piece_sh, get_sh)
+    gather_relay(piece_sh, 12, get_sh)
     gather_finish(piece_sh, get_sh)
     shared_down()
     result = shared_sum[...]
-    for d in range(1, n_sp):
-        wait_recv(ret_buf.at[d], r_send.at[d], r_recv.at[d], {"sp": across(d)})
+    wait_recv(ret_buf.at[0 : n_sp - 1], r_recv.at[0])
     returned = ret_buf[...].reshape(slots, col_dev)
     for c in range(2):
         picked = jnp.dot(pick_buf[c], returned, preferred_element_type=f32)
         result = result + weight_buf[c][:, 0:1] * picked
     out_ref[...] = result.astype(out_ref.dtype)
 
-    for copy in sends:
-        copy.wait_send()
-    for d in range(1, n_sp):
-        pltpu.make_async_remote_copy(
-            src_ref=q_out.at[d],
-            dst_ref=q_buf.at[me_s],
-            send_sem=q_send.at[d],
-            recv_sem=q_recv.at[me_s],
-            device_id={"sp": across(d)},
-            device_id_type=MESH,
-        ).wait_send()
-    for s in range(n_sp):
-
-        @pl.when(me_s != s)
-        def _():
-            for k in range(peers + 1):
-                send_rows(s, k, start=False)
+    hops = 2 * peers + 1
+    for i, ref in enumerate(
+        (
+            kv_buf.at[0 : n_sp - 1],
+            q_buf.at[0 : n_sp - 1],
+            ho_buf.at[0 : peers + 1, 0 : n_sp - 1],
+            ho_buf.at[0:peers, 0],
+            ho_buf.at[0 : peers + 1],
+            hid_buf.at[0:hops],
+            disp_out.at[1:n_sp],
+            peer_out,
+            arr_buf.at[0:hops, near:n_sp],
+            arr_buf.at[0 : peers + 1, 1:near],
+            eh_buf.at[0:hops],
+            ret_buf.at[1:n_sp],
+            sh_buf.at[0:hops],
+        )
+    ):
+        waiter(ref, s_sem.at[i], kv_recv.at[0]).wait_send()
 
 
 def fused_body(
@@ -915,9 +794,7 @@
     cap = (capacity + 15) // 16 * 16
     hid_units = shared_gate.shape[0]
     bf16 = jnp.bfloat16
-    pieces = 4 + 2 * n_sp
-    peer_slots = (n_tp // 2 - 1) * (n_sp // 2)
-    n_gs = 1 + 2 * (n_tp // 2 - 1)
+    peer_slots = (n_tp // 2 - 1) * (n_sp // 2 - 1)
     dma = pltpu.SemaphoreType.DMA
     vmem = pl.BlockSpec(memory_space=pltpu.VMEM)
     hbm = pl.BlockSpec(memory_space=pl.ANY)
@@ -951,21 +828,15 @@
             pltpu.VMEM((2, rows, n_sp * cap), bf16),
             pltpu.VMEM((2, rows, 128), jnp.float32),
             dma((7,)),
+            dma((13,)),
+            dma((n_sp // 2,)),
+            dma((1,)),
+            dma((n_tp,)),
             dma((n_sp,)),
-            dma((n_sp,)),
-            dma((n_sp,)),
-            dma((n_sp,)),
-            dma((n_tp // 2 * n_sp,)),
-            dma((n_tp // 2 * n_sp,)),
-            dma((n_sp,)),
-            dma((n_sp,)),
-            dma((n_sp,)),
-            dma((n_sp,)),
-            dma((pieces * n_gs,)),
-            dma((pieces * n_tp,)),
+            dma((1,)),
+            dma(((3 + 2 * n_sp) * (n_tp // 2),)),
+            dma((peer_slots,)),
             pltpu.VMEM((peer_slots, cap, col_dev), bf16),
-            dma((peer_slots,)),
-            dma((peer_slots,)),
             pltpu.VMEM((rows, col_dev), jnp.float32),
             pltpu.VMEM(query_rows.shape, bf16),
             pltpu.VMEM(key_rows.shape, bf16),
@@ -976,7 +847,7 @@
             pltpu.VMEM((1,) + norm_gain.shape, jnp.float32),
             pltpu.VMEM((topk, rows), jnp.int32),
             pltpu.VMEM((topk, rows), jnp.float32),
-            dma((9,)),
+            dma((7,)),
             pltpu.VMEM(expert_gate.shape[:0:-1], bf16),
             pltpu.VMEM(expert_up.shape[:0:-1], bf16),
             pltpu.VMEM(shared_gate.shape[::-1], bf16),

time: 57.9 us -> 56.1 us (0.969)
  Pallas kernels: 56.7 us -> 55.2 us
    pallas_call x1, Pallas kernels: 56.7 us -> 55.2 us  [fused_body(): pl.pallas_call(functools.partial(layer_kernel, n_sp, n_tp), out_shape=plt...]
where the time goes in v4:
time: 56.1 us; the launch traced here: 55.9 us
  Pallas kernels  55.2 us (98%)
  local copies, waits for them, and re-layouts  0.68 us (1%)
    pallas_call x1, Pallas kernels, fused_body(): pl.pallas_call(functools.partial(layer_kernel, n_sp, n_tp), out_shape=plt...  55.2 us

profile of v4, /device:TPU:0, one launch (start us, length us, event | category | flops | bytes accessed | tf_op | source)
XLA Modules:
  0.0 55.9 jit_solution(183445405825972911)
XLA Ops:
  0.0 55.2 %shard_map.154 = bf16[192,512]{1,0:T(8,128)(2,1)S(1)} custom-call(bf16[192,256]{1,0:T(8,128)(2,1)} %q_hbm.1, bf16[192,256]{1,0:T(8,128)(2,1)} %k_hbm.1, bf16[192,256]{1,0:T(8,128)(2,1)} %v_hbm.1, bf16[192,512]{1,0:T(8,128)(2,1)} %res_hbm.1, f32[1,4]{1,0:T(1,128)} %bitcast.8, f32[1,64]{1,0:T(1,128)} %bitcast.9, f32[1,2048]{1,0:T(1,128)} %bitcast.5, ...), custom_call_target="tpu_custom_call" | custom-call | tf_op jit(solution)/shard_map/pallas_call | solution.py:801
  55.2 0.7 %copy.18 = bf16[192,512]{1,0:T(8,128)(2,1)} copy(bf16[192,512]{1,0:T(8,128)(2,1)S(1)} %shard_map.154) | data formatting | bytes 393216

commit v5 on v4

--- a/solution.py
+++ b/solution.py
@@ -345,9 +345,10 @@
 
     pl.semaphore_wait(barrier, n_sp + n_tp - 2)
 
-    for d in (6, 4, 2, 1):
+    for d in (6, 4, 2, 3, 1):
         dst = across(d)
-        send(kv_out.at[dst // 2], kv_buf.at[me_s], s_sem.at[0], kv_recv.at[d // 2], {"sp": dst})
+        part = kv_recv.at[0 if d % 2 else d // 2]
+        send(kv_out.at[dst // 2], kv_buf.at[me_s], s_sem.at[0], part, {"sp": dst})
 
     def send_queries(ds):
         for d in ds:
@@ -412,7 +413,8 @@
     for d in (6, 4, 2):
         src = across(d)
         wait_recv(kv_buf.at[src], kv_recv.at[d // 2])
-        send(kv_buf.at[src], kv_buf.at[src], s_sem.at[0], kv_recv.at[0], {"sp": across(1)})
+        if d > 2:
+            send(kv_buf.at[src], kv_buf.at[src], s_sem.at[0], kv_recv.at[0], {"sp": across(1)})
         if d == 6:
             send_queries((6, 7, 4, 5))
     for i, (src, dst) in ((3, (w_gate, t_gate)), (4, (w_up, t_up))):

time: 56.1 us -> 55.4 us (0.988)
  Pallas kernels: 55.2 us -> 54.6 us
    pallas_call x1, Pallas kernels: 55.2 us -> 54.6 us  [fused_body(): pl.pallas_call(functools.partial(layer_kernel, n_sp, n_tp), out_shape=plt...]
where the time goes in v5:
time: 55.4 us; the launch traced here: 55.3 us
  Pallas kernels  54.6 us (99%)
  local copies, waits for them, and re-layouts  0.68 us (1%)
    pallas_call x1, Pallas kernels, fused_body(): pl.pallas_call(functools.partial(layer_kernel, n_sp, n_tp), out_shape=plt...  54.6 us

profile of v5, /device:TPU:0, one launch (start us, length us, event | category | flops | bytes accessed | tf_op | source)
XLA Modules:
  0.0 55.3 jit_solution(16315534627200730603)
XLA Ops:
  0.0 54.6 %shard_map.154 = bf16[192,512]{1,0:T(8,128)(2,1)S(1)} custom-call(bf16[192,256]{1,0:T(8,128)(2,1)} %q_hbm.1, bf16[192,256]{1,0:T(8,128)(2,1)} %k_hbm.1, bf16[192,256]{1,0:T(8,128)(2,1)} %v_hbm.1, bf16[192,512]{1,0:T(8,128)(2,1)} %res_hbm.1, f32[1,4]{1,0:T(1,128)} %bitcast.8, f32[1,64]{1,0:T(1,128)} %bitcast.9, f32[1,2048]{1,0:T(1,128)} %bitcast.5, ...), custom_call_target="tpu_custom_call" | custom-call | tf_op jit(solution)/shard_map/pallas_call | solution.py:803
  54.6 0.7 %copy.18 = bf16[192,512]{1,0:T(8,128)(2,1)} copy(bf16[192,512]{1,0:T(8,128)(2,1)S(1)} %shard_map.154) | data formatting | bytes 393216

commit v6 on v5

--- a/solution.py
+++ b/solution.py
@@ -353,7 +353,7 @@
     def send_queries(ds):
         for d in ds:
             dst = across(d)
-            send(q_out.at[dst], q_buf.at[me_s], s_sem.at[1], q_recv.at[0], {"sp": dst})
+            send(q_out.at[dst], q_buf.at[me_s], s_sem.at[1], q_recv.at[d // 4], {"sp": dst})
 
     upper = me_s // (n_sp // 2)
     inner = lax.rem(me_s // 2 + upper, 2)
@@ -414,14 +414,14 @@
         src = across(d)
         wait_recv(kv_buf.at[src], kv_recv.at[d // 2])
         if d > 2:
-            send(kv_buf.at[src], kv_buf.at[src], s_sem.at[0], kv_recv.at[0], {"sp": across(1)})
+            send(kv_buf.at[src], kv_buf.at[src], s_sem.at[0], kv_recv.at[4], {"sp": across(1)})
         if d == 6:
             send_queries((6, 7, 4, 5))
     for i, (src, dst) in ((3, (w_gate, t_gate)), (4, (w_up, t_up))):
         loads[i].wait()
         dst[...] = src[...].T
-    wait_recv(kv_buf.at[0 : n_sp // 2], kv_recv.at[0])
-    wait_recv(q_buf.at[0 : n_sp - 1], q_recv.at[0])
+    wait_recv(kv_buf.at[0:2], kv_recv.at[0])
+    wait_recv(q_buf.at[0:3], q_recv.at[0])
     def send_rows(s, k):
         far = lax.rem(s // batch + upper, 2)
         send(
@@ -480,15 +480,21 @@
                 ho_buf[me_t, s] = o_out[s]
 
 
+    def wait_far():
+        wait_recv(kv_buf.at[0:2], kv_recv.at[4])
+        wait_recv(q_buf.at[0:4], q_recv.at[1])
+
     @pl.when(upper == 1)
     def _():
+        wait_far()
         attend(0)
         attend(batch)
 
     @pl.when(upper == 0)
     def _():
+        attend(0)
+        wait_far()
         attend(batch)
-        attend(0)
 
     split = n_sp // 2
     base = me_s // split * split
@@ -736,8 +742,8 @@
     expert_out(7, 8)
     relay_eh(2, 4)
     relay_eh(6, 7)
+    expert_out(2, 4)
     expert_out(6, 7)
-    expert_out(2, 4)
     gather_relay(piece_sh, 12, get_sh)
     gather_finish(piece_sh, get_sh)
     shared_down()
@@ -831,8 +837,8 @@
             pltpu.VMEM((2, rows, 128), jnp.float32),
             dma((7,)),
             dma((13,)),
-            dma((n_sp // 2,)),
-            dma((1,)),
+            dma((n_sp // 2 + 1,)),
+            dma((2,)),
             dma((n_tp,)),
             dma((n_sp,)),
             dma((1,)),

time: 55.4 us -> 55.1 us (level)
  Pallas kernels: 54.6 us -> 53.9 us
    pallas_call x1, Pallas kernels: 54.6 us -> 53.9 us  [fused_body(): pl.pallas_call(functools.partial(layer_kernel, n_sp, n_tp), out_shape=plt...]
where the time goes in v6:
time: 55.1 us; the launch traced here: 54.6 us
  Pallas kernels  53.9 us (98%)
  local copies, waits for them, and re-layouts  0.68 us (1%)
    pallas_call x1, Pallas kernels, fused_body(): pl.pallas_call(functools.partial(layer_kernel, n_sp, n_tp), out_shape=plt...  53.9 us

profile of v6, /device:TPU:0, one launch (start us, length us, event | category | flops | bytes accessed | tf_op | source)
XLA Modules:
  0.0 54.6 jit_solution(11296027227824986835)
XLA Ops:
  0.0 53.9 %shard_map.154 = bf16[192,512]{1,0:T(8,128)(2,1)S(1)} custom-call(bf16[192,256]{1,0:T(8,128)(2,1)} %q_hbm.1, bf16[192,256]{1,0:T(8,128)(2,1)} %k_hbm.1, bf16[192,256]{1,0:T(8,128)(2,1)} %v_hbm.1, bf16[192,512]{1,0:T(8,128)(2,1)} %res_hbm.1, f32[1,4]{1,0:T(1,128)} %bitcast.8, f32[1,64]{1,0:T(1,128)} %bitcast.9, f32[1,2048]{1,0:T(1,128)} %bitcast.5, ...), custom_call_target="tpu_custom_call" | custom-call | tf_op jit(solution)/shard_map/pallas_call | solution.py:809
  53.9 0.7 %copy.18 = bf16[192,512]{1,0:T(8,128)(2,1)} copy(bf16[192,512]{1,0:T(8,128)(2,1)S(1)} %shard_map.154) | data formatting | bytes 393216
